TPU v7x, 32 devices: a whole 2x2x4 slice. The times are simulated.
32 devices in a mesh: sp: 8 (over z, x), tp: 4 (over y, core).
Axes of the slice: x: 2, y: 2, z: 4, core: 2. Of those that a mesh axis runs over, the one named last changes fastest.
Arguments:
- tokens: bfloat16 [6144, 2048], P(('sp', 'tp')), may hold values from -6 to 6
- norm_gain: bfloat16 [2048], replicated, may hold values from 0.099609375 to 1.8984375
- conv_value_w: bfloat16 [2048, 2048], P('sp', 'tp'), may hold values from -0.125 to 0.125
- conv_gate_w: bfloat16 [2048, 2048], P('sp', 'tp'), may hold values from -0.125 to 0.125
- rnn_input_w: bfloat16 [2048, 2560], P('sp', 'tp'), may hold values from -0.125 to 0.125
- rnn_gate_w: bfloat16 [2048, 2560], P('sp', 'tp'), may hold values from -0.125 to 0.125
- conv_kernel: bfloat16 [31, 2048], P(None, 'tp'), may hold values from -3 to 3
- conv_norm_gain: bfloat16 [2048], P('tp'), may hold values from 0.099609375 to 1.8984375
- conv_norm_shift: bfloat16 [2048], P('tp'), may hold values from -3 to 3
- short_kernel: bfloat16 [4, 2560], P(None, 'tp'), may hold values from -3 to 3
- recur_map: bfloat16 [16, 160, 160], P('tp'), may hold values from -0.5 to 0.5
- input_map: bfloat16 [16, 160, 160], P('tp'), may hold values from -0.5 to 0.5
- decay_param: float32 [2560], P('tp'), may hold values from 4.5 to 16
- decay_shift: float32 [6144, 16], P('sp', 'tp'), may hold values from -1.1 to 0
- initial_state: float32 [2560], P('tp'), may hold values from -5 to 5
- conv_out_w: bfloat16 [2048, 2048], P('tp', 'sp'), may hold values from -0.125 to 0.125
- rnn_out_w: bfloat16 [2560, 2048], P('tp', 'sp'), may hold values from -0.125 to 0.125
Outputs:
- mixed: bfloat16 [6144, 2048], P(('sp', 'tp'))
All inputs are finite; a program needn't handle non-finite values.
Results may differ from a plain program's by a relative error of at most 0.015.
Values may be sent and summed in bfloat16 or wider, within the bound.
A program may use at most 128 MiB of HBM per device.

v0:
```python
import functools

import jax
import jax.numpy as jnp
from jax import lax
from jax.experimental import pallas as pl
from jax.experimental.pallas import tpu as pltpu
from jax.sharding import PartitionSpec as P

EPS = 1e-06
EXPONENT = 8.0


def shifted(x, axis, by):
    peers = lax.axis_size(axis)
    pairs = [(i, i + by) for i in range(peers) if 0 <= i + by < peers]
    return lax.ppermute(x, axis, pairs)


def send_to(src, dst, send, recv, axis, peer):
    return pltpu.make_async_remote_copy(
        src_ref=src,
        dst_ref=dst,
        send_sem=send,
        recv_sem=recv,
        device_id={axis: peer},
        device_id_type=pl.DeviceIdType.MESH,
    )


def project_kernel(n, m, x_ref, w_ref, o_ref, blocks, piece, acc, ring_send, ring_recv, tok_send, tok_recv, own_sem):
    half = n // 2
    me = lax.axis_index("sp")
    lane = lax.axis_index("tp")
    at = jnp.where(me % 2 == 0, me // 2, n - 1 - me // 2)

    def device_at(place):
        place = lax.rem(place + 2 * n, n)
        return jnp.where(place < half, 2 * place, 2 * (n - 1 - place) + 1)

    right = device_at(at + 1)
    left = device_at(at - 1)
    barrier = pltpu.get_barrier_semaphore()
    for peer in (left, right):
        pl.semaphore_signal(barrier, inc=1, device_id={"sp": peer}, device_id_type=pl.DeviceIdType.MESH)
    for i in range(1, m):
        pl.semaphore_signal(
            barrier, inc=1, device_id={"tp": lax.rem(lane + i, m)}, device_id_type=pl.DeviceIdType.MESH
        )
    own_w = pltpu.make_async_copy(w_ref, blocks.at[me], own_sem.at[0])
    own_x = pltpu.make_async_copy(x_ref, piece.at[lane], own_sem.at[1])
    own_w.start()
    own_x.start()
    own_w.wait()
    own_x.wait()
    pl.semaphore_wait(barrier, 2 + m - 1)
    rows = w_ref.shape[0] // 2

    def hop(way, k, part=None):
        slot = device_at(at - (k - 1)) if way == 0 else device_at(at + (k - 1))
        ref = blocks.at[slot] if part is None else blocks.at[slot, pl.ds(part * rows, rows)]
        return send_to(
            ref, ref, ring_send.at[way, k - 1], ring_recv.at[way, k - 1], "sp", right if way == 0 else left
        )

    tokens_out = [
        send_to(x_ref, piece.at[lane], tok_send.at[i - 1], tok_recv.at[i - 1], "tp", lax.rem(lane + i, m))
        for i in range(1, m)
    ]

    def add(slot, first=False):
        def one(j, _):
            here = pl.ds(pl.multiple_of(j * piece.shape[2], piece.shape[2]), piece.shape[2])
            term = jnp.dot(piece[j, slot], blocks[slot], preferred_element_type=jnp.float32)
            acc[here, :] = term if first else acc[here, :] + term
            return 0

        lax.fori_loop(0, m, one, 0)

    hop(0, 1).start()
    hop(1, 1).start()
    for copy in tokens_out:
        copy.start()
    hop(0, 1).wait_recv()
    hop(1, 1).wait_recv()
    hop(0, 2).start()
    hop(1, 2).start()
    for copy in tokens_out:
        copy.wait_recv()
    add(me, True)

    def step(k, _):
        add(device_at(at - (k - 1)))
        add(device_at(at + (k - 1)))
        hop(0, k).wait_recv()
        hop(1, k).wait_recv()

        @pl.when(k + 1 < half)
        def _():
            hop(0, k + 1).start()
            hop(1, k + 1).start()

        return 0

    lax.fori_loop(2, half, step, 0)
    hop(0, half, 0).start()
    hop(1, half, 1).start()
    add(device_at(at - (half - 1)))
    add(device_at(at + (half - 1)))
    hop(0, half, 0).wait_recv()
    hop(1, half, 1).wait_recv()
    add(device_at(at + half))

    def finish(j, _):
        here = pl.ds(pl.multiple_of(j * piece.shape[2], piece.shape[2]), piece.shape[2])
        o_ref[here, :] = acc[here, :].astype(o_ref.dtype)
        return 0

    lax.fori_loop(0, m, finish, 0)

    def sent(k, _):
        hop(0, k).wait_send()
        hop(1, k).wait_send()
        return 0

    lax.fori_loop(1, half, sent, 0)
    hop(0, half, 0).wait_send()
    hop(1, half, 1).wait_send()
    for copy in tokens_out:
        copy.wait_send()


def project(normed, weight):
    n = lax.axis_size("sp")
    m = lax.axis_size("tp")
    rows = normed.shape[0]
    depth, columns = weight.shape
    sliced = normed.reshape(rows, n, depth).transpose(1, 0, 2)
    vmem = pl.BlockSpec(memory_space=pltpu.VMEM)
    return pl.pallas_call(
        functools.partial(project_kernel, n, m),
        out_shape=jax.ShapeDtypeStruct((rows * m, columns), jnp.bfloat16),
        in_specs=[vmem, vmem],
        out_specs=vmem,
        scratch_shapes=[
            pltpu.VMEM((n, depth, columns), jnp.bfloat16),
            pltpu.VMEM((m, n, rows, depth), jnp.bfloat16),
            pltpu.VMEM((rows * m, columns), jnp.float32),
            pltpu.SemaphoreType.DMA((2, n // 2)),
            pltpu.SemaphoreType.DMA((2, n // 2)),
            pltpu.SemaphoreType.DMA((m - 1,)),
            pltpu.SemaphoreType.DMA((m - 1,)),
            pltpu.SemaphoreType.DMA((2,)),
        ],
        cost_estimate=pl.CostEstimate(
            flops=2 * rows * m * depth * n * columns, bytes_accessed=90_000_000, transcendentals=0
        ),
        compiler_params=pltpu.CompilerParams(
            collective_id=0, has_side_effects=True, vmem_limit_bytes=50 * 1024 * 1024
        ),
    )(sliced, weight)


def spread_kernel(n, axis, x_ref, o_ref, send, recv):
    me = lax.axis_index(axis)
    barrier = pltpu.get_barrier_semaphore()

    def greet(i, _):
        pl.semaphore_signal(
            barrier, inc=1, device_id={axis: lax.rem(me + i, n)}, device_id_type=pl.DeviceIdType.MESH
        )
        return 0

    lax.fori_loop(1, n, greet, 0)
    pl.semaphore_wait(barrier, n - 1)

    def copy(i):
        return send_to(x_ref, o_ref.at[me], send.at[i - 1], recv.at[i - 1], axis, lax.rem(me + i, n))

    def start(i, _):
        copy(i).start()
        return 0

    def wait(i, _):
        copy(i).wait()
        return 0

    lax.fori_loop(1, n, start, 0)
    o_ref[pl.ds(me, 1)] = x_ref[...][None]
    lax.fori_loop(1, n, wait, 0)


def spread_over(x, axis, collective_id):
    n = lax.axis_size(axis)
    vmem = pl.BlockSpec(memory_space=pltpu.VMEM)
    return pl.pallas_call(
        functools.partial(spread_kernel, n, axis),
        out_shape=jax.ShapeDtypeStruct((n,) + x.shape, x.dtype),
        in_specs=[vmem],
        out_specs=vmem,
        scratch_shapes=[pltpu.SemaphoreType.DMA((n - 1,)), pltpu.SemaphoreType.DMA((n - 1,))],
        cost_estimate=pl.CostEstimate(flops=0, bytes_accessed=10_000_000, transcendentals=0),
        compiler_params=pltpu.CompilerParams(
            collective_id=collective_id, has_side_effects=True, vmem_limit_bytes=4 * 1024 * 1024
        ),
    )(x)


def scan_kernel(parts, a_ref, b_ref, p_ref, h_ref):
    length, width = a_ref.shape
    run = length // parts
    cols = [slice(None)]

    def one(i, state):
        place = pl.ds(i, parts, stride=run)
        new = []
        for c, (p, h) in zip(cols, state):
            a = a_ref[place, c]
            h = a * h + b_ref[place, c]
            p = a * p
            p_ref[place, c] = p
            h_ref[place, c] = h
            new.append((p, h))
        return new

    first = [(jnp.ones((parts, width), jnp.float32), jnp.zeros((parts, width), jnp.float32)) for _ in cols]
    ends = lax.fori_loop(0, run, one, first)
    for c, (p, h) in zip(cols, ends):
        carry_p = p[0:1]
        carry_h = h[0:1]
        for s in range(1, parts):
            here = pl.ds(s * run, run)
            local_p = p_ref[here, c]
            h_ref[here, c] = h_ref[here, c] + local_p * carry_h
            p_ref[here, c] = local_p * carry_p
            carry_h = p[s : s + 1] * carry_h + h[s : s + 1]
            carry_p = p[s : s + 1] * carry_p


def scan(a, b):
    block = pl.BlockSpec((a.shape[0], 128), lambda c: (0, c))
    return pl.pallas_call(
        functools.partial(scan_kernel, 8),
        grid=(a.shape[1] // 128,),
        out_shape=[jax.ShapeDtypeStruct(a.shape, jnp.float32)] * 2,
        in_specs=[block, block],
        out_specs=[block, block],
        cost_estimate=pl.CostEstimate(flops=4 * a.size, bytes_accessed=16 * a.size, transcendentals=0),
        compiler_params=pltpu.CompilerParams(vmem_limit_bytes=20 * 1024 * 1024),
    )(a, b)


def entering(last_decay, last_drive, initial):
    n = lax.axis_size("sp")
    place = lax.axis_index("sp")
    pair = jnp.stack([last_decay, last_drive])
    gathered = spread_over(jnp.pad(pair, ((0, 6), (0, 0))), "sp", 1)
    state = initial
    for i in range(n):
        state = jnp.where(i < place, gathered[i, 0] * state + gathered[i, 1], state)
    return state


def causal_taps(extended, kernel, length):
    result = jnp.zeros((length, extended.shape[1]), jnp.float32)
    for offset in range(kernel.shape[0]):
        result = result + kernel[offset].astype(jnp.float32) * extended[offset : offset + length]
    return result


def block_diagonal(values, maps):
    heads, size, _ = maps.shape
    rows = [
        jnp.pad(maps[h], ((0, 0), (h * size, (heads - 1 - h) * size))) for h in range(heads)
    ]
    return jnp.dot(values, jnp.concatenate(rows, axis=0), preferred_element_type=jnp.float32)


def local(
    tokens,
    norm_gain,
    conv_value_w,
    conv_gate_w,
    rnn_input_w,
    rnn_gate_w,
    conv_kernel,
    conv_norm_gain,
    conv_norm_shift,
    short_kernel,
    recur_map,
    input_map,
    decay_param,
    decay_shift,
    initial_state,
    conv_out_w,
    rnn_out_w,
):
    as_float = tokens.astype(jnp.float32)
    scale = lax.rsqrt(jnp.mean(as_float * as_float, axis=1, keepdims=True) + EPS)
    normed = (as_float * scale * norm_gain.astype(jnp.float32)).astype(jnp.bfloat16)
    edges = [0]
    for weight in (conv_value_w, conv_gate_w, rnn_input_w, rnn_gate_w):
        edges.append(edges[-1] + weight.shape[1])
    joined = project(
        normed, jnp.concatenate([conv_value_w, conv_gate_w, rnn_input_w, rnn_gate_w], axis=1)
    )
    conv_value, conv_gate, rnn_input, rnn_gate = [
        joined[:, edges[index] : edges[index + 1]] for index in range(4)
    ]
    out_weights = (
        lax.all_gather(conv_out_w, "sp", axis=1, tiled=True),
        lax.all_gather(rnn_out_w, "sp", axis=1, tiled=True),
    )
    length = conv_value.shape[0]
    conv_reach = conv_kernel.shape[0] - 1
    short_reach = short_kernel.shape[0] - 1
    tail = shifted(joined[length - conv_reach :, : edges[3]], "sp", 1)
    value_tail = tail[:, : edges[1]]
    gate_tail = tail[:, edges[1] : edges[2]]
    input_tail = tail[conv_reach - short_reach :, edges[2] :]
    value_ext = jnp.concatenate([value_tail, conv_value], axis=0)
    gate_ext = jnp.concatenate([gate_tail, conv_gate], axis=0)
    input_ext = jnp.concatenate([input_tail, rnn_input], axis=0)
    gated_values = value_ext.astype(jnp.float32) * jax.nn.sigmoid(gate_ext.astype(jnp.float32))
    conv_mixed = causal_taps(gated_values, conv_kernel, length)
    moments = lax.psum(
        (jnp.sum(conv_mixed, axis=1), jnp.sum(conv_mixed * conv_mixed, axis=1)), "tp"
    )
    channels = conv_mixed.shape[1] * lax.axis_size("tp")
    average = moments[0][:, None] / channels
    spread = moments[1][:, None] / channels - average * average
    scaled = (conv_mixed - average) * lax.rsqrt(spread + EPS)
    scaled = scaled * conv_norm_gain.astype(jnp.float32) + conv_norm_shift.astype(jnp.float32)
    conv_hidden = jax.nn.silu(scaled).astype(jnp.bfloat16)
    rnn_short = causal_taps(input_ext.astype(jnp.float32), short_kernel, length).astype(
        jnp.bfloat16
    )
    recur_gate = jax.nn.sigmoid(block_diagonal(rnn_short, recur_map))
    input_gate = jax.nn.sigmoid(block_diagonal(rnn_short, input_map))
    shift_cols = jnp.repeat(decay_shift, recur_map.shape[1], axis=1)
    log_decay = -EXPONENT * recur_gate * jax.nn.softplus(-decay_param)[None, :] + shift_cols
    drive = jnp.sqrt(-jnp.expm1(2.0 * log_decay)) * input_gate * rnn_short.astype(jnp.float32)
    cum_decay, cum_drive = scan(jnp.exp(log_decay), drive)
    state_before = entering(cum_decay[length - 1], cum_drive[length - 1], initial_state)
    states = cum_drive + cum_decay * state_before[None, :]
    rnn_hidden = (states * jax.nn.gelu(rnn_gate.astype(jnp.float32), approximate=True)).astype(
        jnp.bfloat16
    )
    return lax.psum_scatter(
        (
            jnp.dot(conv_hidden, out_weights[0], preferred_element_type=jnp.float32)
            + jnp.dot(rnn_hidden, out_weights[1], preferred_element_type=jnp.float32)
        ).astype(jnp.bfloat16),
        "tp",
        scatter_dimension=0,
        tiled=True,
    )


def solution(mesh):
    return jax.shard_map(
        local,
        mesh=mesh,
        in_specs=(
            P(("sp", "tp"), None),
            P(),
            P("sp", "tp"),
            P("sp", "tp"),
            P("sp", "tp"),
            P("sp", "tp"),
            P(None, "tp"),
            P("tp"),
            P("tp"),
            P(None, "tp"),
            P("tp", None, None),
            P("tp", None, None),
            P("tp"),
            P("sp", "tp"),
            P("tp"),
            P("tp", "sp"),
            P("tp", "sp"),
        ),
        out_specs=P(("sp", "tp"), None),
        check_vma=False,
    )
```

profile of v0, /device:TPU:29, one launch (start us, length us, event | category | flops | bytes accessed | tf_op | source)
XLA Modules:
  0.0 251.5 jit_solution(17598612370740715606)
XLA Ops:
  6.5 0.7 all-gather.5.cloned.1.call-update
  7.3 0.0 all-gather.3.cloned.1.call-start
  7.3 0.7 convert_element_type.127
  8.0 1.4 fusion.17
  9.4 0.0 copy-start.6
  9.4 0.0 copy-start.10
  9.4 0.3 fusion.19
  9.7 0.1 copy.23
  9.7 0.6 copy-done.6
  10.4 0.1 copy-done.7
  10.5 0.1 copy-done.9
  10.5 0.1 copy-done.10
  10.6 0.1 pad_maximum_fusion.w_ref
  10.7 128.6 %shard_map.163 = bf16[768,2304]{1,0:T(8,128)(2,1)} custom-call(bf16[8,192,256]{2,1,0:T(8,128)(2,1)S(1)} %bitcast.59, bf16[256,2304]{1,0:T(8,128)(2,1)S(1)} %pad_maximum_fusion.w_ref), custom_call_target="tpu_custom_call" | custom-call | flops 7247757312 | bytes 90000000 | tf_op jit(solution)/shard_map/pallas_call | solution.py:140
  139.3 0.9 slice.313
  140.2 3.7 %collective-permute-start = (bf16[30,1664]{1,0:T(8,128)(2,1)S(1)}, bf16[30,1664]{1,0:T(8,128)(2,1)S(1)}, u32[]{:S(2)}, u32[]{:S(2)}) collective-permute-start(bf16[30,1664]{1,0:T(8,128)(2,1)S(1)} %slice.313), channel_id=1, source_target_pairs={{0,4},{4,8},{8,12},{12,16},{16,20},{20,24},{24,28},{1,5},{5,9},{9,... | collective-permute-start | bytes 299528 | tf_op jit(solution)/shard_map/ppermute | solution.py:17
  143.9 0.0 all-gather.3.cloned.1.call-update
  144.0 0.0 reduce-scatter.2.cloned.1.call-start
  144.0 0.0 copy-start.11
  144.0 0.0 copy-start.13
  144.0 2.6 %fusion.115 = (bf16[768,512]{1,0:T(8,128)(2,1)}, bf16[768,512]{1,0:T(8,128)(2,1)}) fusion(bf16[768,2304]{1,0:T(8,128)(2,1)} %shard_map.163), kind=kLoop, calls=%fused_computation.227 | loop fusion | bytes 3145728 | tf_op jit(solution)/shard_map/slice | solution.py:308
  146.7 0.6 slice_convert_fusion.29
  147.3 0.7 slice_convert_fusion.30
  148.0 0.1 broadcast_in_dim.2
  148.2 0.0 copy-start.44
  148.2 0.0 copy-start.8
  148.2 0.0 copy-start.47
  148.2 0.0 copy-start.12
  148.2 1.8 copy.20
  150.1 1.1 slice_bitcast_fusion.3
  151.2 0.6 convert_element_type.132
  151.8 0.6 convert_element_type.131
  152.4 0.2 maximum_convert_fusion
  152.7 0.9 fusion.8
  153.5 0.7 copy-done.4
  154.3 1.2 fusion.117
  155.5 2.0 convert_multiply_fusion.3.b_ref
  157.5 8.7 %shard_map.164 = (f32[768,640]{1,0:T(8,128)S(1)}, f32[768,640]{1,0:T(8,128)S(1)}) custom-call(f32[768,640]{1,0:T(8,128)S(1)} %get-tuple-element.79.a_ref, f32[768,640]{1,0:T(8,128)S(1)} %convert_multiply_fusion.3.b_ref), custom_call_target="tpu_custom_call" | custom-call | flops 1966080 | bytes 7864320 | tf_op jit(solution)/shard_map/pallas_call | solution.py:242
  166.3 6.4 %shard_map.165 = f32[8,8,640]{2,1,0:T(8,128)S(1)} custom-call(f32[8,640]{1,0:T(8,128)S(1)} %select_maximum_fusion.x_ref), custom_call_target="tpu_custom_call" | custom-call | bytes 10000000 | tf_op jit(solution)/shard_map/pallas_call | solution.py:196
  173.0 0.6 divide_multiply_fusion
  174.0 7.4 %fusion.113 = (f32[768]{0:T(1024)S(1)}, f32[768]{0:T(1024)S(1)}, f32[768,512]{1,0:T(8,128)}) fusion(f32[798,512]{1,0:T(8,128)S(1)} %divide_multiply_fusion, f32[512]{0:T(512)S(1)} %bitcast.72, f32[512]{0:T(512)S(1)} %bitcast.73, f32[512]{0:T(512)S(1)} %bitcast.75, f32[512]{0:T(512)S(1)} %bitcast.76, f32[512]{0:T(512)S(1)} %bitcast.77, f32[512]{0:T(512)S(1)} %bitcast.78, ...), kind=kLoop, calls=%fused_computation.226 | loop fusion | flops 25164288 | bytes 50401280 | tf_op jit(solution)/shard_map/reduce_sum | solution.py:327
  181.4 9.1 %all-reduce.9 = (f32[768]{0:T(1024)S(1)}, f32[768]{0:T(1024)S(1)}) all-reduce(f32[768]{0:T(1024)S(1)} %get-tuple-element.10, f32[768]{0:T(1024)S(1)} %get-tuple-element.9), channel_id=1, replica_groups=mesh['sp'=8,'tp'=4] {'tp'}, use_global_device_ids=true, to_apply=%region_4.0 | all-reduce | flops 1536 | bytes 12288 | tf_op jit(solution)/shard_map/psum | solution.py:326
  190.5 0.1 slice_reduce_fusion.8
  190.7 0.0 all-gather.5.cloned.1.call-done
  190.7 8.3 %fusion.54 = f32[768,2048]{1,0:T(8,128)} fusion(bf16[640,2048]{1,0:T(8,128)(2,1)} %all-gather.5.cloned.1.call-done, f32[768,640]{1,0:T(8,128)} %copy-done, f32[768,640]{1,0:T(8,128)S(1)} %get-tuple-element.8, bf16[768,2304]{1,0:T(8,128)(2,1)} %shard_map.163, f32[640]{0:T(1024)S(1)} %add_select_fusion), kind=kOutput, calls=%fused_computation.109 | convolution fusion | flops 2019655680 | bytes 13830656 | tf_op jit(solution)/shard_map/dot_general | solution.py:352
  199.0 7.2 %add_convert_fusion = bf16[768,2048]{1,0:T(8,128)(2,1)} fusion(f32[768,2048]{1,0:T(8,128)} %fusion.54, bf16[512,2048]{1,0:T(8,128)(2,1)} %all-gather.3.cloned.1.call-done, f32[768,512]{1,0:T(8,128)S(1)} %copy-done.5, f32[512]{0:T(512)S(1)} %copy-done.45, f32[512]{0:T(512)} %convert_element_type.131, f32[768]{0:T(1024)S(1)} %get-tuple-element.78, ...), kind=kOutput, calls=%fused_computation | convolution fusion | flops 1617297408 | bytes 13117440 | tf_op jit(solution)/shard_map/dot_general | solution.py:351
  206.2 0.0 reduce-scatter.2.cloned.1.call-update
  206.3 38.7 %reduce-scatter.2.cloned.1.call-done = bf16[192,2048]{1,0:T(8,128)(2,1)} async-done(((bf16[768,2048]{1,0:T(8,128)(2,1)}), bf16[192,2048]{1,0:T(8,128)(2,1)}) %reduce-scatter.2.cloned.1.call-update) | async-done | bytes 786448 | tf_op jit(solution)/shard_map/reduce_scatter | solution.py:349
  (99 shorter events, 0.3 us)
Async XLA Ops:
  6.5 2.8 %copy-start.1 = (bf16[192,2048]{1,0:T(8,128)(2,1)S(1)}, bf16[192,2048]{1,0:T(8,128)(2,1)}, u32[]{:S(2)}) copy-start(bf16[192,2048]{1,0:T(8,128)(2,1)} %param.17) | copy-start | bytes 2359300
  6.5 184.1 %all-gather.5.cloned.1.call-start = ((), (), s32[]{:S(2)}) async-start(), calls=%async_computation.2 | async-start | bytes 2949120 | tf_op jit(solution)/shard_map/all_gather | solution.py:312
  7.3 191.7 %all-gather.3.cloned.1.call-start = ((), (), s32[]{:S(2)}) async-start(), calls=%async_computation.1 | async-start | bytes 2359296 | tf_op jit(solution)/shard_map/all_gather | solution.py:311
  9.4 1.0 copy-start.6
  9.4 1.1 copy-start.7
  9.4 1.1 copy-start.9
  9.4 1.2 copy-start.10
  140.2 12.2 %collective-permute-start = (bf16[30,1664]{1,0:T(8,128)(2,1)S(1)}, bf16[30,1664]{1,0:T(8,128)(2,1)S(1)}, u32[]{:S(2)}, u32[]{:S(2)}) collective-permute-start(bf16[30,1664]{1,0:T(8,128)(2,1)S(1)} %slice.313), channel_id=1, source_target_pairs={{0,4},{4,8},{8,12},{12,16},{16,20},{20,24},{24,28},{1,5},{5,9},{9,... | collective-permute-start | bytes 299528 | tf_op jit(solution)/shard_map/ppermute | solution.py:17
  144.0 101.0 %reduce-scatter.2.cloned.1.call-start = ((), (), s32[]{:S(2)}) async-start(), calls=%async_computation.3 | async-start | bytes 3932160 | tf_op jit(solution)/shard_map/reduce_scatter | solution.py:349
  144.0 2.7 %copy-start.11 = (bf16[31,512]{1,0:T(8,128)(2,1)S(1)}, bf16[31,512]{1,0:T(8,128)(2,1)}, u32[]{:S(2)}) copy-start(bf16[31,512]{1,0:T(8,128)(2,1)} %param.23) | copy-start | bytes 95236
  144.0 4.0 %copy-start.13 = (f32[768,4]{0,1:T(4,128)S(1)}, f32[768,4]{0,1:T(4,128)}, u32[]{:S(2)}) copy-start(f32[768,4]{0,1:T(4,128)} %param.30) | copy-start | bytes 36868
  148.2 1.9 copy-start.44
  148.2 1.9 copy-start.8
  148.2 3.0 %copy-start.46 = (bf16[512]{0:T(512)(128)(2,1)S(1)}, bf16[512]{0:T(512)(128)(2,1)}, u32[]{:S(2)}) copy-start(bf16[512]{0:T(512)(128)(2,1)} %param.25) | copy-start | bytes 3076
  148.2 3.6 %copy-start.47 = (bf16[512]{0:T(512)(128)(2,1)S(1)}, bf16[512]{0:T(512)(128)(2,1)}, u32[]{:S(2)}) copy-start(bf16[512]{0:T(512)(128)(2,1)} %param.24) | copy-start | bytes 3076
  148.2 4.2 %copy-start.12 = (bf16[4,640]{1,0:T(4,128)(2,1)S(1)}, bf16[4,640]{1,0:T(4,128)(2,1)}, u32[]{:S(2)}) copy-start(bf16[4,640]{1,0:T(4,128)(2,1)} %param.26) | copy-start | bytes 15364
  150.0 2.4 slice-start
  152.7 1.6 copy-start.4
  157.5 15.3 %copy-start.2 = (bf16[768,512]{1,0:T(8,128)(2,1)S(1)}, bf16[768,512]{1,0:T(8,128)(2,1)}, u32[]{:S(2)}) copy-start(bf16[768,512]{1,0:T(8,128)(2,1)} %get-tuple-element.34) | copy-start | bytes 2359300
  157.5 15.3 %copy-start.3 = (bf16[768,512]{1,0:T(8,128)(2,1)S(1)}, bf16[768,512]{1,0:T(8,128)(2,1)}, u32[]{:S(2)}) copy-start(bf16[768,512]{1,0:T(8,128)(2,1)} %get-tuple-element.35) | copy-start | bytes 2359300
  166.2 7.4 %copy-start = (f32[768,640]{1,0:T(8,128)}, f32[768,640]{1,0:T(8,128)S(1)}, u32[]{:S(2)}) copy-start(f32[768,640]{1,0:T(8,128)S(1)} %get-tuple-element.7) | copy-start | bytes 5898244
  172.8 0.9 copy-start.14
  172.8 0.9 copy-start.15
  172.8 0.9 copy-start.16
  172.8 0.9 copy-start.17
  172.8 0.9 copy-start.18
  172.8 0.9 copy-start.19
  172.8 0.9 copy-start.20
  172.8 0.9 copy-start.21
  172.8 0.9 copy-start.22
  172.8 0.9 copy-start.23
  172.9 0.9 copy-start.24
  172.9 0.9 copy-start.25
  172.9 0.9 copy-start.26
  172.9 0.9 copy-start.27
  172.9 0.9 copy-start.28
  172.9 0.9 copy-start.29
  172.9 0.9 copy-start.30
  172.9 0.9 copy-start.31
  172.9 0.9 copy-start.32
  172.9 0.9 copy-start.33
  173.0 0.9 copy-start.34
  173.0 0.9 copy-start.35
  173.0 0.9 copy-start.36
  173.0 0.9 copy-start.37
  173.9 16.7 %copy-start.43 = (f32[640]{0:T(1024)S(1)}, f32[640]{0:T(1024)}, u32[]{:S(2)}) copy-start(f32[640]{0:T(1024)} %param.31) | copy-start | bytes 7684
  190.6 8.4 %copy-start.5 = (f32[768,512]{1,0:T(8,128)S(1)}, f32[768,512]{1,0:T(8,128)}, u32[]{:S(2)}) copy-start(f32[768,512]{1,0:T(8,128)} %get-tuple-element.33) | copy-start | bytes 4718596
  190.6 8.4 %copy-start.45 = (f32[512]{0:T(512)S(1)}, f32[512]{0:T(512)}, u32[]{:S(2)}) copy-start(f32[512]{0:T(512)} %convert_element_type.132) | copy-start | bytes 6148
  (5 other events, 4.5 us)
Sparse Core Ops, SparseCore 0:
  9.4 84.6 all-gather.4
  144.1 50.1 all-gather.2
  206.4 38.5 reduce-scatter.1
where the time goes:
time: 255 us; the launch traced here: 252 us
  Pallas kernels  144 us (56%)
  waiting for transfers between devices  39.5 us (15%)
  matrix products  18.7 us (7%)
  other arithmetic  14 us (5%)
  between operations  14 us (5%)
  blocking collectives  9.09 us (4%)
  local copies, waits for them, and re-layouts  8.64 us (3%)
  starting transfers between devices  3.77 us (1%)
    pallas_call x1, Pallas kernels, project(): pl.pallas_call(functools.partial(project_kernel, n, m), out_shape=jax.Sha...  129 us
    reduce_scatter x1, waiting for transfers between devices, local(): lax.psum_scatter((jnp.dot(conv_hidden, out_weights[0], preferred_element_...  38.7 us
    psum x1, blocking collectives, local(): lax.psum((jnp.sum(conv_mixed, axis=1), jnp.sum(conv_mixed * conv_mixed, a...  9.09 us
    pallas_call x1, Pallas kernels, scan(): pl.pallas_call(functools.partial(scan_kernel, 8), grid=(a.shape[1] // 128...  8.72 us
    dot_general x1, matrix products, local(): jnp.dot(rnn_hidden, out_weights[1], preferred_element_type=jnp.float32)  8.31 us
    reduce_sum x1, other arithmetic, local(): jnp.sum(conv_mixed, axis=1)  7.42 us
    dot_general x1, matrix products, local(): jnp.dot(conv_hidden, out_weights[0], preferred_element_type=jnp.float32)  7.22 us
    pallas_call x1, Pallas kernels, spread_over(): pl.pallas_call(functools.partial(spread_kernel, n, axis), out_shape=jax.S...  6.42 us
  transfers between devices with their start and end apart: 4, of which 1 were waited for; matrix products, arithmetic and copies ran while one was open for 13% of the time, Pallas kernels for 57%

commit v1 on v0

--- a/solution.py
+++ b/solution.py
@@ -357,9 +357,752 @@
     )
 
 
+def fused_kernel(n, m, dims, *refs):
+    depth, quarter, ca, cr, wid, heads, taps, short = dims
+    (
+        tok_ref, ngain_ref, wv_ref, wg_ref, wri_ref, wrg_ref, wco_ref, wro_ref, pc_hbm, pr_hbm, bd_hbm, sh_hbm,
+        o_ref,
+        NB, X, BC, BI, BG, BO, PC, PR, BD, SH, G, MIX, MS, MR, E, S, Z0, Z1, SHC, RG, HC, HR, SM, SR, PB, R,
+        swap_send, swap_recv, par_send, par_recv, line_send, line_recv, sib_send, sib_recv,
+        tok_send, tok_recv, tokf_send, tokf_recv, halo_send, halo_recv, mom_send, mom_recv,
+        state_send, state_recv, rs_send, rs_recv, tail_sem,
+    ) = refs
+    f32, bf16 = jnp.float32, jnp.bfloat16
+    na, nu = n // 2, m // 2
+    length = quarter * m
+    model = depth * n
+    half = length // 2
+    reach = taps - 1
+    pad = -(-reach // 8) * 8
+    lanes = 128
+    ga, gr = ca // lanes, cr // lanes
+    tiles = length // lanes
+    sp = lax.axis_index("sp")
+    tp = lax.axis_index("tp")
+    a, b = sp // 2, sp % 2
+    u, v = tp // 2, tp % 2
+    same = b == v
+    other = b != v
+    spc = 2 * a + v
+    tpc = 2 * u + b
+
+    def at(s, t):
+        return {"sp": s, "tp": t}
+
+    def where_is(s, t):
+        return at(2 * (s // 2) + t % 2, 2 * (t // 2) + s % 2)
+
+    partner = at(2 * a + v, 2 * u + b)
+    sibling = at(sp, 2 * u + 1 - v)
+
+    def remote(src, dst, send, recv, dev):
+        return pltpu.make_async_remote_copy(
+            src_ref=src, dst_ref=dst, send_sem=send, recv_sem=recv, device_id=dev,
+            device_id_type=pl.DeviceIdType.MESH,
+        )
+
+    barrier = pltpu.get_barrier_semaphore()
+    me = sp * m + tp
+
+    def greet(i, _):
+        to = (me + i) % (n * m)
+        pl.semaphore_signal(barrier, inc=1, device_id=at(to // m, to % m), device_id_type=pl.DeviceIdType.MESH)
+        return 0
+
+    lax.fori_loop(1, n * m, greet, 0)
+
+    bufs = [BC, BI, BG, BO]
+    parts = [
+        [(wv_ref, lambda j: BC.at[j, :, pl.ds(0, ca)]), (wg_ref, lambda j: BC.at[j, :, pl.ds(ca, ca)])],
+        [(wri_ref, lambda j: BI.at[j])],
+        [(wrg_ref, lambda j: BG.at[j])],
+        [(wco_ref, lambda j: BO.at[j, pl.ds(0, ca)]), (wro_ref, lambda j: BO.at[j, pl.ds(ca, cr)])],
+    ]
+    first = [0, 2, 3, 4]
+
+    def each_part(s, act):
+        for p, (src, dst) in enumerate(parts[s]):
+            act(src, dst, first[s] + p)
+
+    def bring_local(s):
+        each_part(s, lambda src, dst, k: pltpu.make_async_copy(src, dst(spc), swap_recv.at[k]).start())
+
+    def swapped(src, dst, k):
+        return remote(src, dst(sp), swap_send.at[k], swap_recv.at[k], partner)
+
+    def bring_remote(s):
+        each_part(s, lambda src, dst, k: swapped(src, dst, k).start())
+
+    def brought(s):
+        @pl.when(same)
+        def _():
+            each_part(s, lambda src, dst, k: pltpu.make_async_copy(src, dst(spc), swap_recv.at[k]).wait())
+
+        @pl.when(other)
+        def _():
+            each_part(s, lambda src, dst, k: swapped(src, dst, k).wait_recv())
+
+    params = [(pc_hbm, PC), (pr_hbm, PR), (bd_hbm, BD)]
+
+    @pl.when(same)
+    def _():
+        for s in range(4):
+            bring_local(s)
+        for k, (src, dst) in enumerate(params):
+            pltpu.make_async_copy(src, dst, par_recv.at[k]).start()
+        pltpu.make_async_copy(sh_hbm, SH, par_recv.at[3]).start()
+
+    gain = ngain_ref[...].astype(f32)
+
+    def norm(i, _):
+        rows = pl.ds(pl.multiple_of(i * 32, 32), 32)
+        t = tok_ref[rows, :].astype(f32)
+        scale = lax.rsqrt(jnp.sum(t * t, axis=1, keepdims=True) * (1.0 / model) + EPS)
+        y = (t * scale * gain).astype(bf16)
+        NB[rows, :] = y
+
+        @pl.when(same)
+        def _():
+            X[tp, rows, :] = y
+
+        return 0
+
+    lax.fori_loop(0, quarter // 32, norm, 0)
+    pl.semaphore_wait(barrier, n * m - 1)
+
+    def param_send(k):
+        return remote(params[k][0], params[k][1], par_send.at[k], par_recv.at[k], sibling)
+
+    shift_send = remote(sh_hbm, SH, par_send.at[3], par_recv.at[3], partner)
+
+    @pl.when(other)
+    def _():
+        bring_remote(0)
+        bring_remote(1)
+
+    tok_peer = remote(
+        NB, X.at[tp], tok_send.at[0], tok_recv.at[v], at(2 * a + 1 - b, 2 * u + b)
+    )
+    tok_sib = remote(NB, X.at[tp], tok_send.at[1], tok_recv.at[v], sibling)
+
+    @pl.when(other)
+    def _():
+        tok_sib.start()
+
+    tok_peer.start()
+
+    @pl.when(same)
+    def _():
+        for k in range(3):
+            param_send(k).start()
+
+    @pl.when(other)
+    def _():
+        bring_remote(2)
+        bring_remote(3)
+        shift_send.start()
+
+    def block(s, j):
+        return bufs[s].at[j]
+
+    def up(s, o):
+        ref = block(s, 2 * o + v)
+        return remote(ref, ref, line_send.at[s, 0, o], line_recv.at[s, o], at(2 * a + 2 + b, tp))
+
+    def down(s, o):
+        ref = block(s, 2 * o + v)
+        return remote(ref, ref, line_send.at[s, 1, o], line_recv.at[s, o], at(2 * a - 2 + b, tp))
+
+    def across(s, o, core):
+        ref = block(s, 2 * o + core)
+        return remote(ref, ref, sib_send.at[s, o], sib_recv.at[s, o], sibling)
+
+    def own(s):
+        brought(s)
+
+        @pl.when(a + 1 < na)
+        def _():
+            up(s, a).start()
+
+        @pl.when(a > 0)
+        def _():
+            down(s, a).start()
+
+        across(s, a, v).start()
+
+    def step(s, k):
+        @pl.when(a - k >= 0)
+        def _():
+            up(s, a - k).wait_recv()
+
+            @pl.when(a + 1 < na)
+            def _():
+                up(s, a - k).start()
+
+            across(s, a - k, v).start()
+
+        @pl.when(a + k < na)
+        def _():
+            down(s, a + k).wait_recv()
+
+            @pl.when(a > 0)
+            def _():
+                down(s, a + k).start()
+
+            across(s, a + k, v).start()
+
+    def crossed(s):
+        def one(o, _):
+            across(s, o, 1 - v).wait_recv()
+            return 0
+
+        lax.fori_loop(0, na, one, 0)
+
+    def tok_from(c):
+        q = 2 * u + c
+        return remote(NB, X.at[q], tok_send.at[0], tok_recv.at[c], sibling)
+
+    def tok_forward(i, uu):
+        ref = X.at[pl.ds(2 * uu, 2)]
+        return remote(ref, ref, tokf_send.at[i - 1], tokf_recv.at[i - 1], at(sp, 2 * ((u + i) % nu) + v))
+
+    own(0)
+    own(1)
+    if na > 1:
+        step(0, 1)
+    for c in range(2):
+
+        @pl.when(jnp.logical_or(other, v != c))
+        def _():
+            tok_from(c).wait_recv()
+
+    for i in range(1, nu):
+        tok_forward(i, u).start()
+    for k in range(2, na):
+        step(0, k)
+    own(2)
+    if na > 1:
+        step(1, 1)
+
+    @pl.when(same)
+    def _():
+        for k, (src, dst) in enumerate(params):
+            pltpu.make_async_copy(src, dst, par_recv.at[k]).wait()
+        pltpu.make_async_copy(sh_hbm, SH, par_recv.at[3]).wait()
+
+    @pl.when(other)
+    def _():
+        for k in range(3):
+            param_send(k).wait_recv()
+        shift_send.wait_recv()
+
+    for i in range(1, nu):
+        tok_forward(i, (u - i + nu) % nu).wait_recv()
+    crossed(0)
+
+    chunk = 256
+    cols_a = ca // chunk
+
+    def tokens_half(r):
+        return X[pl.ds(r * nu, nu)].reshape(half, model)
+
+    def conv_project(i, _):
+        r, j = i // cols_a, i % cols_a
+        x = tokens_half(r)
+        at_v = pl.ds(pl.multiple_of(j * chunk, chunk), chunk)
+        at_g = pl.ds(pl.multiple_of(ca + j * chunk, chunk), chunk)
+        val = jnp.dot(x, BC[:, :, at_v].reshape(model, chunk), preferred_element_type=f32).astype(bf16)
+        gate = jnp.dot(x, BC[:, :, at_g].reshape(model, chunk), preferred_element_type=f32).astype(bf16)
+        out = val.astype(f32) * jax.nn.sigmoid(gate.astype(f32))
+        rows = pl.ds(pl.multiple_of(pad + r * half, 8), half)
+        for g in range(chunk // lanes):
+            G[j * (chunk // lanes) + g, rows, :] = out[:, g * lanes : (g + 1) * lanes]
+        return 0
+
+    total = 2 * cols_a
+    lax.fori_loop(0, total // 2, conv_project, 0)
+    if na > 2:
+        step(1, 2)
+    lax.fori_loop(total // 2, total, conv_project, 0)
+    behind = where_is(spc + 1, tpc)
+    conv_halo = remote(
+        G.at[:, pl.ds(length, pad)], G.at[:, pl.ds(0, pad)], halo_send.at[0], halo_recv.at[0], behind
+    )
+    rnn_halo = remote(
+        E.at[:, pl.ds(length, 8)], E.at[:, pl.ds(0, 8)], halo_send.at[1], halo_recv.at[1], behind
+    )
+
+    @pl.when(spc + 1 < n)
+    def _():
+        conv_halo.start()
+
+    for k in range(3, na):
+        step(1, k)
+    own(3)
+
+    @pl.when(spc == 0)
+    def _():
+        G[:, 0:pad, :] = jnp.zeros((ga, pad, lanes), f32)
+        E[:, 0:8, :] = jnp.zeros((gr, 8, lanes), f32)
+
+    @pl.when(spc > 0)
+    def _():
+        conv_halo.wait_recv()
+
+    lane = lax.broadcasted_iota(jnp.int32, (lanes, lanes), 1)
+    sub = lax.broadcasted_iota(jnp.int32, (lanes, lanes), 0)
+
+    def convolve(i, _):
+        t0 = pl.multiple_of(i * lanes, lanes)
+        sums = jnp.zeros((lanes, lanes), f32)
+        squares = jnp.zeros((lanes, lanes), f32)
+        for g in range(ga):
+            here = slice(g * lanes, (g + 1) * lanes)
+            acc = jnp.zeros((lanes, lanes), f32)
+            for k in range(taps):
+                acc = acc + PC[k : k + 1, here] * G[g, pl.ds(t0 + (pad - reach + k), lanes), :]
+            MIX[g, pl.ds(t0, lanes), :] = acc
+            sums = sums + acc
+            squares = squares + acc * acc
+        s1 = jnp.sum(sums, axis=1, keepdims=True)
+        s2 = jnp.sum(squares, axis=1, keepdims=True)
+        both = jnp.where(lane == 0, s1, jnp.where(lane == 1, s2, 0.0))
+        MS[i] = both.T[0:8, :]
+        return 0
+
+    lax.fori_loop(0, tiles // 2, convolve, 0)
+    if na > 1:
+        step(2, 1)
+    lax.fori_loop(tiles // 2, tiles, convolve, 0)
+
+    def moments(i):
+        return remote(
+            MS, MR.at[i - 1], mom_send.at[i - 1], mom_recv.at[i - 1], where_is(spc, (tpc + i) % m)
+        )
+
+    for k in range(2, min(3, na)):
+        step(2, k)
+    for i in range(1, m):
+        moments(i).start()
+    crossed(1)
+
+    spans = []
+    left = 0
+    while left < cr:
+        spans.append((left, min(chunk, cr - left)))
+        left += chunk
+
+    def input_project(r, _):
+        x = tokens_half(r)
+        rows = pl.ds(pl.multiple_of(8 + r * half, 8), half)
+        for lo, size in spans:
+            out = jnp.dot(x, BI[:, :, lo : lo + size].reshape(model, size), preferred_element_type=f32)
+            out = out.astype(bf16).astype(f32)
+            for g in range(size // lanes):
+                E[lo // lanes + g, rows, :] = out[:, g * lanes : (g + 1) * lanes]
+        return 0
+
+    lax.fori_loop(0, 2, input_project, 0)
+
+    @pl.when(spc + 1 < n)
+    def _():
+        rnn_halo.start()
+
+    for k in range(3, na):
+        step(2, k)
+
+    def shift_columns(i, _):
+        full = jnp.concatenate([SH[i], jnp.zeros((lanes - 8, lanes), f32)], axis=0)
+        SHC[pl.ds(pl.multiple_of(i * lanes, lanes), lanes), :] = full.T
+        return 0
+
+    lax.fori_loop(0, tiles, shift_columns, 0)
+
+    @pl.when(spc > 0)
+    def _():
+        rnn_halo.wait_recv()
+
+    def short_conv(i, _):
+        t0 = pl.multiple_of(i * lanes, lanes)
+        for g in range(gr):
+            here = slice(g * lanes, (g + 1) * lanes)
+            acc = jnp.zeros((lanes, lanes), f32)
+            for k in range(short):
+                acc = acc + PR[k : k + 1, here] * E[g, pl.ds(t0 + (8 - short + 1 + k), lanes), :]
+            S[pl.ds(t0, lanes), here] = acc.astype(bf16)
+        return 0
+
+    lax.fori_loop(0, tiles, short_conv, 0)
+
+    def gate_maps(r, _):
+        rows = pl.ds(pl.multiple_of(r * half, half), half)
+        s = S[rows, :]
+        Z0[rows, :] = jnp.dot(s, BD[0], preferred_element_type=f32)
+        Z1[rows, :] = jnp.dot(s, BD[1], preferred_element_type=f32)
+        return 0
+
+    lax.fori_loop(0, 2, gate_maps, 0)
+    if na > 1:
+        step(3, 1)
+
+    size = 32
+    subs = size // 8
+    head = cr // heads
+    lane32 = lax.broadcasted_iota(jnp.int32, (size, lanes), 1)
+    row8 = lax.broadcasted_iota(jnp.int32, (subs, 8, lanes), 1)
+
+    def recur(i, carry):
+        rows = pl.ds(pl.multiple_of(i * size, size), size)
+        shc = SHC[rows, :]
+        new = []
+        for g in range(gr):
+            here = slice(g * lanes, (g + 1) * lanes)
+            shift = None
+            for h in reversed(range((g * lanes) // head, (g * lanes + lanes - 1) // head + 1)):
+                col = jnp.broadcast_to(shc[:, h : h + 1], (size, lanes))
+                shift = col if shift is None else jnp.where(lane32 < (h + 1) * head - g * lanes, col, shift)
+            log_decay = PR[short : short + 1, here] * jax.nn.sigmoid(Z0[rows, here]) + shift
+            t = jnp.tanh(log_decay)
+            drive = jnp.sqrt((-2.0 * t) / (1.0 - t)) * jax.nn.sigmoid(Z1[rows, here])
+            drive = drive * S[rows, here].astype(f32)
+            p = jnp.exp(log_decay).reshape(subs, 8, lanes)
+            h_ = drive.reshape(subs, 8, lanes)
+            for d in (1, 2, 4):
+                keep = row8 >= d
+                ps = jnp.where(keep, pltpu.roll(p, d, 1), 1.0)
+                hs = jnp.where(keep, pltpu.roll(h_, d, 1), 0.0)
+                h_ = p * hs + h_
+                p = p * ps
+            Z0[rows, here] = p.reshape(size, lanes)
+            Z1[rows, here] = h_.reshape(size, lanes)
+            pc, hc = carry[g]
+            for q in range(subs):
+                pe = p[q, 7:8, :]
+                hc = pe * hc + h_[q, 7:8, :]
+                pc = pe * pc
+            new.append((pc, hc))
+        return new
+
+    start = [(jnp.ones((1, lanes), f32), jnp.zeros((1, lanes), f32)) for _ in range(gr)]
+    ends = lax.fori_loop(0, length // size, recur, start)
+    for g in range(gr):
+        here = slice(g * lanes, (g + 1) * lanes)
+        SM[0:1, here] = ends[g][0]
+        SM[1:2, here] = ends[g][1]
+    SM[2:8, :] = jnp.zeros((6, cr), f32)
+
+    def state_to(i):
+        return remote(SM, SR.at[spc], state_send.at[i - 1], state_recv.at[i - 1], where_is(spc + i, tpc))
+
+    def state_from(i):
+        return remote(SM, SR.at[spc - i], state_send.at[i - 1], state_recv.at[i - 1], where_is(spc, tpc))
+
+    for i in range(1, n):
+
+        @pl.when(spc + i < n)
+        def _():
+            state_to(i).start()
+
+    crossed(2)
+
+    def gate_project(r, _):
+        x = tokens_half(r)
+        rows = pl.ds(pl.multiple_of(r * half, half), half)
+        for lo, size_ in spans:
+            out = jnp.dot(x, BG[:, :, lo : lo + size_].reshape(model, size_), preferred_element_type=f32)
+            RG[rows, lo : lo + size_] = out.astype(bf16)
+        return 0
+
+    lax.fori_loop(0, 2, gate_project, 0)
+    for i in range(1, m):
+        moments(i).wait_recv()
+
+    def conv_finish(i, _):
+        tot = MS[i]
+        for p in range(m - 1):
+            tot = tot + MR[p, i]
+        average = tot[0:1, :] * (1.0 / (ca * m))
+        spread = tot[1:2, :] * (1.0 / (ca * m)) - average * average
+        inv = lax.rsqrt(spread + EPS)
+        full = jnp.where(sub == 0, average, jnp.where(sub == 1, inv, 0.0)).T
+        rows = pl.ds(pl.multiple_of(i * lanes, lanes), lanes)
+        av, iv = full[:, 0:1], full[:, 1:2]
+        for g in range(ga):
+            here = slice(g * lanes, (g + 1) * lanes)
+            y = (MIX[g, rows, :] - av) * iv * PC[taps : taps + 1, here] + PC[taps + 1 : taps + 2, here]
+            HC[rows, here] = (y * jax.nn.sigmoid(y)).astype(bf16)
+        return 0
+
+    lax.fori_loop(0, tiles, conv_finish, 0)
+    for i in range(1, n):
+
+        @pl.when(spc - i >= 0)
+        def _():
+            state_from(i).wait_recv()
+
+    def enter(i, state):
+        return SR[i, 0:1, :] * state + SR[i, 1:2, :]
+
+    before = lax.fori_loop(0, spc, enter, PR[short + 1 : short + 2, :])
+
+    def rnn_finish(i, carry):
+        rows = pl.ds(pl.multiple_of(i * size, size), size)
+        new = []
+        for g in range(gr):
+            here = slice(g * lanes, (g + 1) * lanes)
+            p = Z0[rows, here]
+            h_ = Z1[rows, here]
+            hc = carry[g]
+            outs = []
+            for q in range(subs):
+                st = p[8 * q : 8 * q + 8] * hc + h_[8 * q : 8 * q + 8]
+                outs.append(st)
+                hc = st[7:8, :]
+            new.append(hc)
+            st = jnp.concatenate(outs, axis=0)
+            gate = RG[rows, here].astype(f32)
+            HR[rows, here] = (st * jax.nn.gelu(gate, approximate=True)).astype(bf16)
+        return new
+
+    lax.fori_loop(0, length // size, rnn_finish, [before[:, g * lanes : (g + 1) * lanes] for g in range(gr)])
+
+    def out_copy(j, q):
+        return remote(PB.at[j, q], R.at[tpc, j], rs_send.at[j, q], rs_recv.at[j, tpc], at(2 * a + v, q))
+
+    def out_from(j, t):
+        return remote(PB.at[j, 0], R.at[t, j], rs_send.at[j, 0], rs_recv.at[j, t], sibling)
+
+    def out_block(j):
+        y = jnp.dot(HC[...], BO[j, 0:ca], preferred_element_type=f32)
+        y = (y + jnp.dot(HR[...], BO[j, ca : ca + cr], preferred_element_type=f32)).astype(bf16)
+        PB[j] = y.reshape(m, quarter, wid)
+        for q in range(m):
+            mine = jnp.logical_and(same, tp == q)
+
+            @pl.when(jnp.logical_not(mine))
+            def _():
+                out_copy(j, q).start()
+
+            @pl.when(mine)
+            def _():
+                R[tpc, j] = y[q * quarter : (q + 1) * quarter]
+
+    def settle(j):
+        y = jnp.zeros((quarter, wid), f32)
+        for t in range(m):
+
+            @pl.when(jnp.logical_or(other, tpc != t))
+            def _():
+                out_from(j, t).wait_recv()
+
+        for t in range(m):
+            y = y + R[t, j].astype(f32)
+        o_ref[:, pl.ds(pl.multiple_of(j * wid, wid), wid)] = y.astype(o_ref.dtype)
+
+    def each_block(k, act):
+        def one(i, _):
+            o = jnp.where(i < 2, a - k, a + k)
+            core = jnp.where(i % 2 == 0, v, 1 - v)
+            ok = jnp.where(i < 2, a - k >= 0, jnp.logical_and(a + k < na, k > 0))
+
+            @pl.when(ok)
+            def _():
+                act(o, 2 * o + core, i % 2)
+
+            return 0
+
+        lax.fori_loop(0, 4, one, 0)
+
+    def produce(o, j, far):
+        @pl.when(far == 1)
+        def _():
+            across(3, o, 1 - v).wait_recv()
+
+        out_block(j)
+
+    def outer(k, _):
+        @pl.when(k >= 2)
+        def _():
+            step(3, k)
+
+        each_block(k, produce)
+
+        @pl.when(k >= 1)
+        def _():
+            each_block(k - 1, lambda o, j, far: settle(j))
+
+        return 0
+
+    lax.fori_loop(0, na, outer, 0)
+    each_block(na - 1, lambda o, j, far: settle(j))
+
+    def drain(o, _):
+        for s in range(4):
+
+            @pl.when(jnp.logical_and(o <= a, a + 1 < na))
+            def _():
+                up(s, o).wait_send()
+
+            @pl.when(jnp.logical_and(o >= a, a > 0))
+            def _():
+                down(s, o).wait_send()
+
+            across(s, o, v).wait_send()
+        return 0
+
+    lax.fori_loop(0, na, drain, 0)
+
+    @pl.when(other)
+    def _():
+        for s in range(4):
+            each_part(s, lambda src, dst, k: swapped(src, dst, k).wait_send())
+        shift_send.wait_send()
+        tok_sib.wait_send()
+
+    @pl.when(same)
+    def _():
+        for k in range(3):
+            param_send(k).wait_send()
+
+    tok_peer.wait_send()
+    for i in range(1, nu):
+        tok_forward(i, u).wait_send()
+
+    @pl.when(spc + 1 < n)
+    def _():
+        conv_halo.wait_send()
+        rnn_halo.wait_send()
+
+    for i in range(1, m):
+        moments(i).wait_send()
+    for i in range(1, n):
+
+        @pl.when(spc + i < n)
+        def _():
+            state_to(i).wait_send()
+
+    def drain_out(j, _):
+        for q in range(m):
+
+            @pl.when(jnp.logical_not(jnp.logical_and(same, tp == q)))
+            def _():
+                out_copy(j, q).wait_send()
+
+        return 0
+
+    lax.fori_loop(0, n, drain_out, 0)
+
+
+def fused(
+    tokens, norm_gain, conv_value_w, conv_gate_w, rnn_input_w, rnn_gate_w, conv_kernel, conv_norm_gain,
+    conv_norm_shift, short_kernel, recur_map, input_map, decay_param, decay_shift, initial_state, conv_out_w,
+    rnn_out_w,
+):
+    n = lax.axis_size("sp")
+    m = lax.axis_size("tp")
+    f32, bf16 = jnp.float32, jnp.bfloat16
+    quarter, model = tokens.shape
+    depth, ca = conv_value_w.shape
+    cr = rnn_input_w.shape[1]
+    wid = conv_out_w.shape[1]
+    heads = recur_map.shape[0]
+    taps, short = conv_kernel.shape[0], short_kernel.shape[0]
+    length = quarter * m
+    tiles = length // 128
+    pad = -(-(taps - 1) // 8) * 8
+    pc_rows = -(-(taps + 2) // 8) * 8
+    pc = jnp.concatenate([conv_kernel, conv_norm_gain[None], conv_norm_shift[None]], axis=0).astype(f32)
+    pc = jnp.pad(pc, ((0, pc_rows - taps - 2), (0, 0)))
+    rate = -EXPONENT * jax.nn.softplus(-decay_param)
+    pr = jnp.concatenate([short_kernel.astype(f32), rate[None], initial_state[None]], axis=0)
+    pr_rows = -(-(short + 2) // 8) * 8
+    pr = jnp.pad(pr, ((0, pr_rows - short - 2), (0, 0)))
+    bd = jnp.stack([spread_heads(recur_map), spread_heads(input_map)])
+    sh = decay_shift.T.reshape(heads, tiles, 128).transpose(1, 0, 2)
+    sh = jnp.pad(sh, ((0, 0), (0, 8 - heads), (0, 0)))
+    vmem = pl.BlockSpec(memory_space=pltpu.VMEM)
+    anyw = pl.BlockSpec(memory_space=pl.ANY)
+    na, nu = n // 2, m // 2
+    dma = pltpu.SemaphoreType.DMA
+    dims = (depth, quarter, ca, cr, wid, heads, taps, short)
+    return pl.pallas_call(
+        functools.partial(fused_kernel, n, m, dims),
+        out_shape=jax.ShapeDtypeStruct((quarter, model), bf16),
+        in_specs=[vmem, vmem] + [anyw] * 10,
+        out_specs=vmem,
+        scratch_shapes=[
+            pltpu.VMEM((quarter, model), bf16),
+            pltpu.VMEM((m, quarter, model), bf16),
+            pltpu.VMEM((n, depth, 2 * ca), bf16),
+            pltpu.VMEM((n, depth, cr), bf16),
+            pltpu.VMEM((n, depth, cr), bf16),
+            pltpu.VMEM((n, ca + cr, wid), bf16),
+            pltpu.VMEM((pc_rows, ca), f32),
+            pltpu.VMEM((pr_rows, cr), f32),
+            pltpu.VMEM((2, cr, cr), bf16),
+            pltpu.VMEM((tiles, 8, 128), f32),
+            pltpu.VMEM((ca // 128, pad + length, 128), f32),
+            pltpu.VMEM((ca // 128, length, 128), f32),
+            pltpu.VMEM((tiles, 8, 128), f32),
+            pltpu.VMEM((m - 1, tiles, 8, 128), f32),
+            pltpu.VMEM((cr // 128, 8 + length, 128), f32),
+            pltpu.VMEM((length, cr), bf16),
+            pltpu.VMEM((length, cr), f32),
+            pltpu.VMEM((length, cr), f32),
+            pltpu.VMEM((length, 128), f32),
+            pltpu.VMEM((length, cr), bf16),
+            pltpu.VMEM((length, ca), bf16),
+            pltpu.VMEM((length, cr), bf16),
+            pltpu.VMEM((8, cr), f32),
+            pltpu.VMEM((n, 8, cr), f32),
+            pltpu.VMEM((n, m, quarter, wid), bf16),
+            pltpu.VMEM((m, n, quarter, wid), bf16),
+            dma((6,)), dma((6,)), dma((4,)), dma((4,)),
+            dma((4, 2, na)), dma((4, na)), dma((4, na)), dma((4, na)),
+            dma((2,)), dma((2,)), dma((max(nu - 1, 1),)), dma((max(nu - 1, 1),)),
+            dma((2,)), dma((2,)), dma((m - 1,)), dma((m - 1,)),
+            dma((n - 1,)), dma((n - 1,)), dma((n, m)), dma((n, m)), dma((1,)),
+        ],
+        cost_estimate=pl.CostEstimate(
+            flops=2 * length * (model * 2 * (ca + cr) + (ca + cr) * model), bytes_accessed=10_000_000,
+            transcendentals=0,
+        ),
+        compiler_params=pltpu.CompilerParams(
+            collective_id=7, has_side_effects=True, vmem_limit_bytes=60 * 1024 * 1024
+        ),
+    )(
+        tokens, norm_gain[None], conv_value_w, conv_gate_w, rnn_input_w, rnn_gate_w, conv_out_w, rnn_out_w,
+        pc, pr, bd, sh,
+    )
+
+
+def spread_heads(maps):
+    heads, size, _ = maps.shape
+    rows = [jnp.pad(maps[h], ((0, 0), (h * size, (heads - 1 - h) * size))) for h in range(heads)]
+    return jnp.concatenate(rows, axis=0)
+
+
+def fits(n, m, args):
+    quarter, model = args[0].shape
+    depth, ca = args[2].shape
+    cr = args[4].shape[1]
+    wid = args[15].shape[1]
+    heads = args[10].shape[0]
+    return (
+        n % 2 == 0 and m % 2 == 0 and wid % 128 == 0 and ca % 256 == 0 and cr % 128 == 0 and depth % 16 == 0
+        and quarter % 32 == 0 and (quarter * m) % 256 == 0 and heads <= 8
+    )
+
+
+def whole_program(*args):
+    n = lax.axis_size("sp")
+    m = lax.axis_size("tp")
+    return fused(*args) if fits(n, m, args) else local(*args)
+
+
 def solution(mesh):
     return jax.shard_map(
-        local,
+        whole_program,
         mesh=mesh,
         in_specs=(
             P(("sp", "tp"), None),

time: 255 us -> 166 us (0.65); the launches traced: 252 us -> 165 us
  waiting for transfers between devices: 39.5 us -> 0 us
  matrix products: 18.7 us -> 0 us
  between operations: 14 us -> 0.14 us
  Pallas kernels: 144 us -> 157 us
  other arithmetic: 14 us -> 2.98 us
  blocking collectives: 9.09 us -> 0 us
  starting transfers between devices: 3.77 us -> 0 us
  local copies, waits for them, and re-layouts: 8.64 us -> 5.42 us
    reduce_scatter x1 -> x0, waiting for transfers between devices: 38.7 us -> none  [local(): lax.psum_scatter((jnp.dot(conv_hidden, out_weights[0], preferred_element_...]
    dot_general x4 -> x0, matrix products: 18.7 us -> none  [the longest x1 8.31 us: local(): jnp.dot(rnn_hidden, out_weights[1], preferred_element_type=jnp.float32)]
    pallas_call x3 -> x1, Pallas kernels: 144 us -> 157 us  [fused(): pl.pallas_call(functools.partial(fused_kernel, n, m, dims), out_shape=jax...]
    psum x1 -> x0, blocking collectives: 9.09 us -> none  [local(): lax.psum((jnp.sum(conv_mixed, axis=1), jnp.sum(conv_mixed * conv_mixed, a...]
    reduce_sum x2 -> x0, other arithmetic: 8.79 us -> none  [the longest x1 7.42 us: local(): jnp.sum(conv_mixed, axis=1)]
    ppermute x1 -> x0, starting transfers between devices: 3.69 us -> none  [shifted(): return lax.ppermute(x, axis, pairs)]
    slice x9 -> x0, local copies, waits for them, and re-layouts: 3.69 us -> none  [the longest x3 2.63 us: local(): joined[:, edges[index]:edges[index + 1]]]
    convert_element_type x6 -> x1, other arithmetic: 3.16 us -> 0.01 us  [fused(): short_kernel.astype(f32)]
  transfers between devices with their start and end apart: 4 -> 0, of which waited for: 1 -> 0; matrix products, arithmetic and copies ran while one was open for 13% -> 0% of each run, Pallas kernels for 57% -> 0%
where the time goes in v1:
time: 166 us; the launch traced here: 165 us
  Pallas kernels  157 us (95%)
  local copies, waits for them, and re-layouts  5.42 us (3%)
  other arithmetic  2.98 us (2%)
    pallas_call x1, Pallas kernels, fused(): pl.pallas_call(functools.partial(fused_kernel, n, m, dims), out_shape=jax...  157 us

profile of v1, /device:TPU:29, one launch (start us, length us, event | category | flops | bytes accessed | tf_op | source)
XLA Modules:
  0.0 165.3 jit_solution(11293468031766478299)
XLA Ops:
  0.0 1.0 slice_bitcast_fusion.3
  1.0 1.0 slice_bitcast_fusion.7
  2.1 0.3 fusion.13
  2.4 0.0 copy-start.6
  2.4 0.0 copy-start.7
  2.4 0.0 copy-start
  2.4 0.0 copy-start.2
  2.5 0.0 copy-start.4
  2.5 0.0 copy-start.5
  2.5 0.0 copy-start.1
  2.5 0.0 copy-start.3
  2.5 1.4 pad_maximum_fusion.refs_10_
  3.9 0.0 copy-done.6
  3.9 0.0 copy-done.7
  3.9 0.0 copy-done
  3.9 0.7 fusion.23.refs_8_
  4.5 0.0 copy-done.2
  4.6 0.0 copy-done.4
  4.6 0.0 copy-done.5
  4.6 0.6 select_maximum_fusion.refs_9_
  5.2 0.0 copy-done.1
  5.2 0.6 pad.53.refs_11_
  5.8 0.0 copy-done.3
  5.8 0.6 broadcast_in_dim.15.refs_1_
  6.4 156.8 %shard_map.163 = bf16[192,2048]{1,0:T(8,128)(2,1)} custom-call(bf16[192,2048]{1,0:T(8,128)(2,1)} %refs_0_.1, bf16[1,2048]{1,0:T(2,128)(2,1)} %broadcast_in_dim.15.refs_1_, bf16[256,512]{1,0:T(8,128)(2,1)} %refs_2_.1, bf16[256,512]{1,0:T(8,128)(2,1)} %refs_3_.1, bf16[256,640]{1,0:T(8,128)(2,1)} %refs_4_.1, bf16[256,640]{1,0:T(8,128)(2,1)} %refs_5_.1, ...), custom_call_target="tpu_custom_call" | custom-call | flops 10871635968 | bytes 10000000 | tf_op jit(solution)/shard_map/pallas_call | solution.py:1028
  163.2 2.1 %copy.19 = bf16[192,2048]{1,0:T(8,128)(2,1)} copy(bf16[192,2048]{1,0:T(8,128)(2,1)} %shard_map.163) | data formatting | bytes 1572864
  (6 shorter events, 0.0 us)
Async XLA Ops:
  2.4 1.5 copy-start.6
  2.4 1.5 copy-start.7
  2.4 1.5 copy-start
  2.4 2.1 %copy-start.2 = (bf16[4,640]{1,0:T(4,128)(2,1)S(1)}, bf16[4,640]{1,0:T(4,128)(2,1)}, u32[]{:S(2)}) copy-start(bf16[4,640]{1,0:T(4,128)(2,1)} %param.26) | copy-start | bytes 15364
  2.5 2.1 %copy-start.4 = (f32[640]{0:T(1024)S(1)}, f32[640]{0:T(1024)}, u32[]{:S(2)}) copy-start(f32[640]{0:T(1024)} %param.29) | copy-start | bytes 7684
  2.5 2.1 %copy-start.5 = (f32[640]{0:T(1024)S(1)}, f32[640]{0:T(1024)}, u32[]{:S(2)}) copy-start(f32[640]{0:T(1024)} %param.31) | copy-start | bytes 7684
  2.5 2.7 %copy-start.1 = (f32[768,4]{0,1:T(4,128)S(1)}, f32[768,4]{0,1:T(4,128)}, u32[]{:S(2)}) copy-start(f32[768,4]{0,1:T(4,128)} %param.30) | copy-start | bytes 36868
  2.5 3.3 %copy-start.3 = (bf16[2048]{0:T(1024)(128)(2,1)S(1)}, bf16[2048]{0:T(1024)(128)(2,1)}, u32[]{:S(2)}) copy-start(bf16[2048]{0:T(1024)(128)(2,1)} %param.18) | copy-start | bytes 12292

commit v2 on v1

--- a/solution.py
+++ b/solution.py
@@ -360,12 +360,13 @@
 def fused_kernel(n, m, dims, *refs):
     depth, quarter, ca, cr, wid, heads, taps, short = dims
     (
-        tok_ref, ngain_ref, wv_ref, wg_ref, wri_ref, wrg_ref, wco_ref, wro_ref, pc_hbm, pr_hbm, bd_hbm, sh_hbm,
+        tok_ref, ngain_hbm, wv_ref, wg_ref, wri_ref, wrg_ref, wco_ref, wro_ref, taps_hbm, cgain_hbm, cshift_hbm,
+        short_hbm, rmap_hbm, imap_hbm, decay_hbm, init_hbm, sh_hbm,
         o_ref,
-        NB, X, BC, BI, BG, BO, PC, PR, BD, SH, G, MIX, MS, MR, E, S, Z0, Z1, SHC, RG, HC, HR, SM, SR, PB, R,
-        swap_send, swap_recv, par_send, par_recv, line_send, line_recv, sib_send, sib_recv,
+        TB, NGB, NB, X, BC, BI, BG, BO, KB, CGB, CSB, SKB, RM, DPB, ISB, PK, PC, BD, SH, G, MIX, MS, MR, E, S, Z0, Z1, SHC, RG, HC, HR, SM, SR, PB, R,
+        own_sem, swap_send, swap_recv, par_send, par_recv, line_send, line_recv, sib_send, sib_recv,
         tok_send, tok_recv, tokf_send, tokf_recv, halo_send, halo_recv, mom_send, mom_recv,
-        state_send, state_recv, rs_send, rs_recv, tail_sem,
+        state_send, state_recv, rs_send, rs_recv,
     ) = refs
     f32, bf16 = jnp.float32, jnp.bfloat16
     na, nu = n // 2, m // 2
@@ -409,16 +410,34 @@
         pl.semaphore_signal(barrier, inc=1, device_id=at(to // m, to % m), device_id_type=pl.DeviceIdType.MESH)
         return 0
 
+    gets = [
+        pltpu.make_async_copy(tok_ref, TB, own_sem.at[0]),
+        pltpu.make_async_copy(ngain_hbm, NGB, own_sem.at[1]),
+    ]
+    for get in gets:
+        get.start()
     lax.fori_loop(1, n * m, greet, 0)
 
-    bufs = [BC, BI, BG, BO]
+    hw = wid // 2
+    bufs = [
+        lambda o, core: BC.at[2 * o + core],
+        lambda o, core: BI.at[2 * o + core],
+        lambda o, core: BG.at[2 * o + core],
+        lambda o, core: BO.at[0, o, core],
+        lambda o, core: BO.at[1, o, core],
+    ]
     parts = [
         [(wv_ref, lambda j: BC.at[j, :, pl.ds(0, ca)]), (wg_ref, lambda j: BC.at[j, :, pl.ds(ca, ca)])],
         [(wri_ref, lambda j: BI.at[j])],
         [(wrg_ref, lambda j: BG.at[j])],
-        [(wco_ref, lambda j: BO.at[j, pl.ds(0, ca)]), (wro_ref, lambda j: BO.at[j, pl.ds(ca, cr)])],
     ]
-    first = [0, 2, 3, 4]
+    for e in range(2):
+        here = pl.ds(e * hw, hw)
+        parts.append([
+            (wco_ref.at[:, here], lambda j, e=e: BO.at[e, j // 2, j % 2, pl.ds(0, ca)]),
+            (wro_ref.at[:, here], lambda j, e=e: BO.at[e, j // 2, j % 2, pl.ds(ca, cr)]),
+        ])
+    first = [0, 2, 3, 4, 6]
 
     def each_part(s, act):
         for p, (src, dst) in enumerate(parts[s]):
@@ -442,21 +461,27 @@
         def _():
             each_part(s, lambda src, dst, k: swapped(src, dst, k).wait_recv())
 
-    params = [(pc_hbm, PC), (pr_hbm, PR), (bd_hbm, BD)]
+    params = [
+        (taps_hbm, KB), (cgain_hbm, CGB), (cshift_hbm, CSB), (short_hbm, SKB), (decay_hbm, DPB), (init_hbm, ISB),
+        (rmap_hbm, RM.at[0]), (imap_hbm, RM.at[1]),
+    ]
+    np_ = len(params)
 
     @pl.when(same)
     def _():
-        for s in range(4):
+        for s in range(5):
             bring_local(s)
         for k, (src, dst) in enumerate(params):
             pltpu.make_async_copy(src, dst, par_recv.at[k]).start()
-        pltpu.make_async_copy(sh_hbm, SH, par_recv.at[3]).start()
-
-    gain = ngain_ref[...].astype(f32)
+        pltpu.make_async_copy(sh_hbm, SH, par_recv.at[np_]).start()
+
+    for get in gets:
+        get.wait()
+    gain = NGB[...].astype(f32).reshape(1, model)
 
     def norm(i, _):
         rows = pl.ds(pl.multiple_of(i * 32, 32), 32)
-        t = tok_ref[rows, :].astype(f32)
+        t = TB[rows, :].astype(f32)
         scale = lax.rsqrt(jnp.sum(t * t, axis=1, keepdims=True) * (1.0 / model) + EPS)
         y = (t * scale * gain).astype(bf16)
         NB[rows, :] = y
@@ -473,82 +498,84 @@
     def param_send(k):
         return remote(params[k][0], params[k][1], par_send.at[k], par_recv.at[k], sibling)
 
-    shift_send = remote(sh_hbm, SH, par_send.at[3], par_recv.at[3], partner)
+    shift_send = remote(sh_hbm, SH, par_send.at[np_], par_recv.at[np_], partner)
+
+    tok_peer = remote(NB, X.at[tp], tok_send.at[0], tok_recv.at[v], at(2 * a + 1 - b, 2 * u + b))
+    tok_sib = remote(NB, X.at[tp], tok_send.at[1], tok_recv.at[v], sibling)
 
     @pl.when(other)
     def _():
         bring_remote(0)
-        bring_remote(1)
-
-    tok_peer = remote(
-        NB, X.at[tp], tok_send.at[0], tok_recv.at[v], at(2 * a + 1 - b, 2 * u + b)
-    )
-    tok_sib = remote(NB, X.at[tp], tok_send.at[1], tok_recv.at[v], sibling)
-
-    @pl.when(other)
-    def _():
-        tok_sib.start()
-
-    tok_peer.start()
 
     @pl.when(same)
     def _():
-        for k in range(3):
+        tok_peer.start()
+        for k in range(np_):
             param_send(k).start()
 
-    @pl.when(other)
-    def _():
-        bring_remote(2)
-        bring_remote(3)
-        shift_send.start()
-
-    def block(s, j):
-        return bufs[s].at[j]
+    def block(s, o, core):
+        return bufs[s](o, core) if isinstance(s, int) else BO.at[s - 3, o, core]
 
     def up(s, o):
-        ref = block(s, 2 * o + v)
+        ref = block(s, o, v)
         return remote(ref, ref, line_send.at[s, 0, o], line_recv.at[s, o], at(2 * a + 2 + b, tp))
 
     def down(s, o):
-        ref = block(s, 2 * o + v)
+        ref = block(s, o, v)
         return remote(ref, ref, line_send.at[s, 1, o], line_recv.at[s, o], at(2 * a - 2 + b, tp))
 
     def across(s, o, core):
-        ref = block(s, 2 * o + core)
+        ref = block(s, o, core)
         return remote(ref, ref, sib_send.at[s, o], sib_recv.at[s, o], sibling)
 
-    def own(s):
+    low = a < na // 2
+
+    def inward(s, k, act):
+        @pl.when(jnp.logical_and(low, a - k >= 0))
+        def _():
+            act(up(s, a - k))
+
+        @pl.when(jnp.logical_and(jnp.logical_not(low), a + k < na))
+        def _():
+            act(down(s, a + k))
+
+    def outward(s, k, act):
+        @pl.when(jnp.logical_and(jnp.logical_and(low, a > 0), a + k < na))
+        def _():
+            act(down(s, a + k))
+
+        @pl.when(jnp.logical_and(jnp.logical_and(jnp.logical_not(low), a + 1 < na), a - k >= 0))
+        def _():
+            act(up(s, a - k))
+
+    window = 2
+    going_in, going_out = [], []
+
+    def push(way, order, s, k):
+        if len(order) >= window:
+            way(*order[-window], lambda c: c.wait_send())
+        way(s, k, lambda c: c.start())
+        order.append((s, k))
+
+    def push_in(s, k):
+        push(inward, going_in, s, k)
+
+    def push_out(s, k):
+        push(outward, going_out, s, k)
+
+    def hold(s):
         brought(s)
-
-        @pl.when(a + 1 < na)
-        def _():
-            up(s, a).start()
-
-        @pl.when(a > 0)
-        def _():
-            down(s, a).start()
-
         across(s, a, v).start()
 
-    def step(s, k):
+    def take(s, k):
         @pl.when(a - k >= 0)
         def _():
             up(s, a - k).wait_recv()
-
-            @pl.when(a + 1 < na)
-            def _():
-                up(s, a - k).start()
-
             across(s, a - k, v).start()
 
         @pl.when(a + k < na)
         def _():
             down(s, a + k).wait_recv()
-
-            @pl.when(a > 0)
-            def _():
-                down(s, a + k).start()
-
             across(s, a + k, v).start()
 
     def crossed(s):
@@ -562,42 +589,112 @@
         q = 2 * u + c
         return remote(NB, X.at[q], tok_send.at[0], tok_recv.at[c], sibling)
 
-    def tok_forward(i, uu):
-        ref = X.at[pl.ds(2 * uu, 2)]
-        return remote(ref, ref, tokf_send.at[i - 1], tokf_recv.at[i - 1], at(sp, 2 * ((u + i) % nu) + v))
-
-    own(0)
-    own(1)
-    if na > 1:
-        step(0, 1)
-    for c in range(2):
-
+    def tok_forward(i, uu, c):
+        ref = X.at[2 * uu + c]
+        return remote(ref, ref, tokf_send.at[i - 1, c], tokf_recv.at[i - 1, c], at(sp, 2 * ((u + i) % nu) + v))
+
+    at_end = jnp.logical_or(a == 0, a == na - 1)
+
+    def mids(f):
+        return pl.when(jnp.logical_not(at_end))(f)
+
+    def ends(f):
+        return pl.when(at_end)(f)
+
+    def token_relay(c):
         @pl.when(jnp.logical_or(other, v != c))
         def _():
             tok_from(c).wait_recv()
 
-    for i in range(1, nu):
-        tok_forward(i, u).start()
-    for k in range(2, na):
-        step(0, k)
-    own(2)
-    if na > 1:
-        step(1, 1)
+        for i in range(1, nu):
+            tok_forward(i, u, c).start()
+
+    hold(0)
+    push_in(0, 0)
+    push_out(0, 0)
+
+    @pl.when(other)
+    def _():
+        bring_remote(1)
+        tok_sib.start()
+        tok_peer.start()
+
+    hold(1)
+    push_in(1, 0)
+    push_out(1, 0)
+    take(0, 1)
+    push_in(0, 1)
+    push_out(0, 1)
+    token_relay(v)
+    take(1, 1)
+    push_in(1, 1)
+    push_out(1, 1)
+    token_relay(1 - v)
+
+    @pl.when(other)
+    def _():
+        bring_remote(2)
+        shift_send.start()
+        bring_remote(3)
+        bring_remote(4)
+
+    take(0, 2)
+    push_out(0, 2)
+
+    @mids
+    def _():
+        take(1, 2)
+        push_out(1, 2)
+
+    hold(2)
+    push_in(2, 0)
 
     @pl.when(same)
     def _():
         for k, (src, dst) in enumerate(params):
             pltpu.make_async_copy(src, dst, par_recv.at[k]).wait()
-        pltpu.make_async_copy(sh_hbm, SH, par_recv.at[3]).wait()
+        pltpu.make_async_copy(sh_hbm, SH, par_recv.at[np_]).wait()
 
     @pl.when(other)
     def _():
-        for k in range(3):
+        for k in range(np_):
             param_send(k).wait_recv()
         shift_send.wait_recv()
 
+    head = cr // heads
+    PC[0:taps, :] = KB[...].astype(f32)
+    PK[0:1, 0:ca] = CGB[...].astype(f32).reshape(1, ca)
+    PK[1:2, 0:ca] = CSB[...].astype(f32).reshape(1, ca)
+    PK[2 : 2 + short, 0:cr] = SKB[...].astype(f32)
+    x = -DPB[...].reshape(1, cr)
+    z = jnp.exp(-jnp.abs(x))
+    z = z / (2.0 + z)
+    z2 = z * z
+    series = jnp.full_like(z, 1.0 / 17.0)
+    for k in range(15, 0, -2):
+        series = series * z2 + 1.0 / k
+    PK[2 + short : 3 + short, 0:cr] = -EXPONENT * (jnp.maximum(x, 0.0) + 2.0 * z * series)
+    PK[3 + short : 4 + short, 0:cr] = ISB[...].reshape(1, cr)
+    for g in range(2):
+        BD[g] = jnp.zeros((cr, cr), bf16)
+        for h in range(heads):
+            BD[g, h * head : (h + 1) * head, h * head : (h + 1) * head] = RM[g, h]
+
+    def shift_columns(i, _):
+        cols = SH[:, pl.ds(pl.multiple_of(i * lanes, lanes), lanes)]
+        full = jnp.concatenate([cols, jnp.zeros((lanes - heads, lanes), f32)], axis=0)
+        SHC[pl.ds(pl.multiple_of(i * lanes, lanes), lanes), :] = full.T
+        return 0
+
+    lax.fori_loop(0, tiles, shift_columns, 0)
+
+    @ends
+    def _():
+        take(0, 3)
+
     for i in range(1, nu):
-        tok_forward(i, (u - i + nu) % nu).wait_recv()
+        for c in range(2):
+            tok_forward(i, (u - i + nu) % nu, c).wait_recv()
     crossed(0)
 
     chunk = 256
@@ -619,11 +716,7 @@
             G[j * (chunk // lanes) + g, rows, :] = out[:, g * lanes : (g + 1) * lanes]
         return 0
 
-    total = 2 * cols_a
-    lax.fori_loop(0, total // 2, conv_project, 0)
-    if na > 2:
-        step(1, 2)
-    lax.fori_loop(total // 2, total, conv_project, 0)
+    lax.fori_loop(0, 2 * cols_a, conv_project, 0)
     behind = where_is(spc + 1, tpc)
     conv_halo = remote(
         G.at[:, pl.ds(length, pad)], G.at[:, pl.ds(0, pad)], halo_send.at[0], halo_recv.at[0], behind
@@ -636,9 +729,16 @@
     def _():
         conv_halo.start()
 
-    for k in range(3, na):
-        step(1, k)
-    own(3)
+    @mids
+    def _():
+        push_out(2, 0)
+        take(2, 1)
+
+    push_in(2, 1)
+    hold(3)
+    push_in(3, 0)
+    hold(4)
+    push_in(4, 0)
 
     @pl.when(spc == 0)
     def _():
@@ -648,6 +748,10 @@
     @pl.when(spc > 0)
     def _():
         conv_halo.wait_recv()
+
+    @mids
+    def _():
+        push_out(2, 1)
 
     lane = lax.broadcasted_iota(jnp.int32, (lanes, lanes), 1)
     sub = lax.broadcasted_iota(jnp.int32, (lanes, lanes), 0)
@@ -670,20 +774,26 @@
         MS[i] = both.T[0:8, :]
         return 0
 
-    lax.fori_loop(0, tiles // 2, convolve, 0)
-    if na > 1:
-        step(2, 1)
-    lax.fori_loop(tiles // 2, tiles, convolve, 0)
+    lax.fori_loop(0, tiles, convolve, 0)
 
     def moments(i):
         return remote(
             MS, MR.at[i - 1], mom_send.at[i - 1], mom_recv.at[i - 1], where_is(spc, (tpc + i) % m)
         )
 
-    for k in range(2, min(3, na)):
-        step(2, k)
     for i in range(1, m):
         moments(i).start()
+
+    @mids
+    def _():
+        take(2, 2)
+        push_out(2, 2)
+
+    @ends
+    def _():
+        take(1, 2)
+        take(1, 3)
+
     crossed(1)
 
     spans = []
@@ -708,16 +818,6 @@
     def _():
         rnn_halo.start()
 
-    for k in range(3, na):
-        step(2, k)
-
-    def shift_columns(i, _):
-        full = jnp.concatenate([SH[i], jnp.zeros((lanes - 8, lanes), f32)], axis=0)
-        SHC[pl.ds(pl.multiple_of(i * lanes, lanes), lanes), :] = full.T
-        return 0
-
-    lax.fori_loop(0, tiles, shift_columns, 0)
-
     @pl.when(spc > 0)
     def _():
         rnn_halo.wait_recv()
@@ -728,7 +828,7 @@
             here = slice(g * lanes, (g + 1) * lanes)
             acc = jnp.zeros((lanes, lanes), f32)
             for k in range(short):
-                acc = acc + PR[k : k + 1, here] * E[g, pl.ds(t0 + (8 - short + 1 + k), lanes), :]
+                acc = acc + PK[2 + k : 3 + k, here] * E[g, pl.ds(t0 + (8 - short + 1 + k), lanes), :]
             S[pl.ds(t0, lanes), here] = acc.astype(bf16)
         return 0
 
@@ -742,12 +842,16 @@
         return 0
 
     lax.fori_loop(0, 2, gate_maps, 0)
-    if na > 1:
-        step(3, 1)
+
+    @mids
+    def _():
+        take(3, 1)
+        push_out(3, 0)
+
+    push_in(3, 1)
 
     size = 32
     subs = size // 8
-    head = cr // heads
     lane32 = lax.broadcasted_iota(jnp.int32, (size, lanes), 1)
     row8 = lax.broadcasted_iota(jnp.int32, (subs, 8, lanes), 1)
 
@@ -761,7 +865,7 @@
             for h in reversed(range((g * lanes) // head, (g * lanes + lanes - 1) // head + 1)):
                 col = jnp.broadcast_to(shc[:, h : h + 1], (size, lanes))
                 shift = col if shift is None else jnp.where(lane32 < (h + 1) * head - g * lanes, col, shift)
-            log_decay = PR[short : short + 1, here] * jax.nn.sigmoid(Z0[rows, here]) + shift
+            log_decay = PK[2 + short : 3 + short, here] * jax.nn.sigmoid(Z0[rows, here]) + shift
             t = jnp.tanh(log_decay)
             drive = jnp.sqrt((-2.0 * t) / (1.0 - t)) * jax.nn.sigmoid(Z1[rows, here])
             drive = drive * S[rows, here].astype(f32)
@@ -784,11 +888,11 @@
         return new
 
     start = [(jnp.ones((1, lanes), f32), jnp.zeros((1, lanes), f32)) for _ in range(gr)]
-    ends = lax.fori_loop(0, length // size, recur, start)
+    last = lax.fori_loop(0, length // size, recur, start)
     for g in range(gr):
         here = slice(g * lanes, (g + 1) * lanes)
-        SM[0:1, here] = ends[g][0]
-        SM[1:2, here] = ends[g][1]
+        SM[0:1, here] = last[g][0]
+        SM[1:2, here] = last[g][1]
     SM[2:8, :] = jnp.zeros((6, cr), f32)
 
     def state_to(i):
@@ -803,17 +907,13 @@
         def _():
             state_to(i).start()
 
-    crossed(2)
-
-    def gate_project(r, _):
-        x = tokens_half(r)
-        rows = pl.ds(pl.multiple_of(r * half, half), half)
-        for lo, size_ in spans:
-            out = jnp.dot(x, BG[:, :, lo : lo + size_].reshape(model, size_), preferred_element_type=f32)
-            RG[rows, lo : lo + size_] = out.astype(bf16)
-        return 0
-
-    lax.fori_loop(0, 2, gate_project, 0)
+
+    @mids
+    def _():
+        take(4, 1)
+        push_out(3, 1)
+
+    push_in(4, 1)
     for i in range(1, m):
         moments(i).wait_recv()
 
@@ -829,11 +929,28 @@
         av, iv = full[:, 0:1], full[:, 1:2]
         for g in range(ga):
             here = slice(g * lanes, (g + 1) * lanes)
-            y = (MIX[g, rows, :] - av) * iv * PC[taps : taps + 1, here] + PC[taps + 1 : taps + 2, here]
+            y = (MIX[g, rows, :] - av) * iv * PK[0:1, here] + PK[1:2, here]
             HC[rows, here] = (y * jax.nn.sigmoid(y)).astype(bf16)
         return 0
 
     lax.fori_loop(0, tiles, conv_finish, 0)
+    @ends
+    def _():
+        take(2, 1)
+        take(2, 2)
+        take(2, 3)
+
+    crossed(2)
+
+    def gate_project(r, _):
+        x = tokens_half(r)
+        rows = pl.ds(pl.multiple_of(r * half, half), half)
+        for lo, size_ in spans:
+            out = jnp.dot(x, BG[:, :, lo : lo + size_].reshape(model, size_), preferred_element_type=f32)
+            RG[rows, lo : lo + size_] = out.astype(bf16)
+        return 0
+
+    lax.fori_loop(0, 2, gate_project, 0)
     for i in range(1, n):
 
         @pl.when(spc - i >= 0)
@@ -843,7 +960,7 @@
     def enter(i, state):
         return SR[i, 0:1, :] * state + SR[i, 1:2, :]
 
-    before = lax.fori_loop(0, spc, enter, PR[short + 1 : short + 2, :])
+    before = lax.fori_loop(0, spc, enter, PK[3 + short : 4 + short, 0:cr])
 
     def rnn_finish(i, carry):
         rows = pl.ds(pl.multiple_of(i * size, size), size)
@@ -866,107 +983,132 @@
 
     lax.fori_loop(0, length // size, rnn_finish, [before[:, g * lanes : (g + 1) * lanes] for g in range(gr)])
 
-    def out_copy(j, q):
-        return remote(PB.at[j, q], R.at[tpc, j], rs_send.at[j, q], rs_recv.at[j, tpc], at(2 * a + v, q))
-
-    def out_from(j, t):
-        return remote(PB.at[j, 0], R.at[t, j], rs_send.at[j, 0], rs_recv.at[j, t], sibling)
-
-    def out_block(j):
-        y = jnp.dot(HC[...], BO[j, 0:ca], preferred_element_type=f32)
-        y = (y + jnp.dot(HR[...], BO[j, ca : ca + cr], preferred_element_type=f32)).astype(bf16)
-        PB[j] = y.reshape(m, quarter, wid)
+    @mids
+    def _():
+        take(3, 2)
+        push_out(3, 2)
+
+    def out_copy(e, o, q):
+        return remote(
+            PB.at[e, o, q], R.at[tpc, e, o], rs_send.at[e, o, q], rs_recv.at[e, o, tpc], at(2 * a + v, q)
+        )
+
+    def out_from(e, o, t):
+        return remote(PB.at[e, o, 0], R.at[t, e, o], rs_send.at[e, o, 0], rs_recv.at[e, o, t], sibling)
+
+    def produce(e, o):
+        across(3 + e, o, 1 - v).wait_recv()
+        w = jnp.concatenate([BO[e, o, 0], BO[e, o, 1]], axis=1)
+        y = jnp.dot(HC[...], w[0:ca], preferred_element_type=f32)
+        y = (y + jnp.dot(HR[...], w[ca : ca + cr], preferred_element_type=f32)).astype(bf16)
+        PB[e, o] = y.reshape(m, quarter, wid)
         for q in range(m):
             mine = jnp.logical_and(same, tp == q)
 
             @pl.when(jnp.logical_not(mine))
             def _():
-                out_copy(j, q).start()
+                out_copy(e, o, q).start()
 
             @pl.when(mine)
             def _():
-                R[tpc, j] = y[q * quarter : (q + 1) * quarter]
-
-    def settle(j):
-        y = jnp.zeros((quarter, wid), f32)
+                R[tpc, e, o] = y[q * quarter : (q + 1) * quarter]
+
+    def settle(e, o):
         for t in range(m):
 
             @pl.when(jnp.logical_or(other, tpc != t))
             def _():
-                out_from(j, t).wait_recv()
-
-        for t in range(m):
-            y = y + R[t, j].astype(f32)
-        o_ref[:, pl.ds(pl.multiple_of(j * wid, wid), wid)] = y.astype(o_ref.dtype)
-
-    def each_block(k, act):
-        def one(i, _):
-            o = jnp.where(i < 2, a - k, a + k)
-            core = jnp.where(i % 2 == 0, v, 1 - v)
-            ok = jnp.where(i < 2, a - k >= 0, jnp.logical_and(a + k < na, k > 0))
+                out_from(e, o, t).wait_recv()
+
+        y = R[0, e, o].astype(f32)
+        for t in range(1, m):
+            y = y + R[t, e, o].astype(f32)
+        y = y.astype(o_ref.dtype)
+        for c in range(2):
+            lo = pl.multiple_of((2 * o + c) * wid + e * hw, hw)
+            o_ref[:, pl.ds(lo, hw)] = y[:, c * hw : (c + 1) * hw]
+
+    def each_origin(i, act):
+        e = jnp.where(jnp.logical_or(i == 1, i > na), 1, 0)
+        k = jnp.where(i < 2, 0, jnp.where(i <= na, i - 1, i - na))
+
+        def one(t, _):
+            o = jnp.where(t == 0, a - k, a + k)
+            ok = jnp.where(t == 0, o >= 0, jnp.logical_and(o < na, k > 0))
 
             @pl.when(ok)
             def _():
-                act(o, 2 * o + core, i % 2)
+                act(e, o)
 
             return 0
 
-        lax.fori_loop(0, 4, one, 0)
-
-    def produce(o, j, far):
-        @pl.when(far == 1)
-        def _():
-            across(3, o, 1 - v).wait_recv()
-
-        out_block(j)
-
-    def outer(k, _):
-        @pl.when(k >= 2)
-        def _():
-            step(3, k)
-
-        each_block(k, produce)
-
-        @pl.when(k >= 1)
-        def _():
-            each_block(k - 1, lambda o, j, far: settle(j))
-
-        return 0
-
-    lax.fori_loop(0, na, outer, 0)
-    each_block(na - 1, lambda o, j, far: settle(j))
+        def ready():
+            @pl.when(jnp.logical_and(at_end, k > 0))
+            def _():
+                take(3 + e, k)
+
+        return ready, lambda: lax.fori_loop(0, 2, one, 0)
+
+    def outer(i, _):
+        ready, run = each_origin(i, produce)
+        ready()
+
+        @pl.when(jnp.logical_and(jnp.logical_not(at_end), i == na + 2))
+        def _():
+            take(4, 2)
+
+        run()
+
+        @mids
+        def _():
+            for stage, k in ((na - 1, 0), (na + 1, 1), (na + 2, 2)):
+
+                @pl.when(i == stage)
+                def _():
+                    push_out(4, k)
+
+        @pl.when(jnp.logical_and(at_end, i >= 1))
+        def _():
+            each_origin(i - 1, settle)[1]()
+
+        return 0
+
+    lax.fori_loop(0, 2 * na, outer, 0)
+
+    def conclude(i, _):
+        each_origin(i, settle)[1]()
+        return 0
+
+    lax.fori_loop(jnp.where(at_end, 2 * na - 1, 0), 2 * na, conclude, 0)
 
     def drain(o, _):
-        for s in range(4):
-
-            @pl.when(jnp.logical_and(o <= a, a + 1 < na))
-            def _():
-                up(s, o).wait_send()
-
-            @pl.when(jnp.logical_and(o >= a, a > 0))
-            def _():
-                down(s, o).wait_send()
-
+        for s in range(5):
             across(s, o, v).wait_send()
         return 0
 
+    assert len(going_in) == 10 and len(going_out) == 15
     lax.fori_loop(0, na, drain, 0)
 
+    for way, order in ((inward, going_in), (outward, going_out)):
+        for one in order[-window:]:
+            way(*one, lambda c: c.wait_send())
+
     @pl.when(other)
     def _():
-        for s in range(4):
+        for s in range(5):
             each_part(s, lambda src, dst, k: swapped(src, dst, k).wait_send())
         shift_send.wait_send()
         tok_sib.wait_send()
 
     @pl.when(same)
     def _():
-        for k in range(3):
+        for k in range(np_):
             param_send(k).wait_send()
 
     tok_peer.wait_send()
     for i in range(1, nu):
-        tok_forward(i, u).wait_send()
+        for c in range(2):
+            tok_forward(i, u, c).wait_send()
 
     @pl.when(spc + 1 < n)
     def _():
@@ -981,16 +1123,17 @@
         def _():
             state_to(i).wait_send()
 
-    def drain_out(j, _):
-        for q in range(m):
-
-            @pl.when(jnp.logical_not(jnp.logical_and(same, tp == q)))
-            def _():
-                out_copy(j, q).wait_send()
-
-        return 0
-
-    lax.fori_loop(0, n, drain_out, 0)
+    def drain_out(o, _):
+        for e in range(2):
+            for q in range(m):
+
+                @pl.when(jnp.logical_not(jnp.logical_and(same, tp == q)))
+                def _():
+                    out_copy(e, o, q).wait_send()
+
+        return 0
+
+    lax.fori_loop(0, na, drain_out, 0)
 
 
 def fused(
@@ -1010,16 +1153,8 @@
     length = quarter * m
     tiles = length // 128
     pad = -(-(taps - 1) // 8) * 8
-    pc_rows = -(-(taps + 2) // 8) * 8
-    pc = jnp.concatenate([conv_kernel, conv_norm_gain[None], conv_norm_shift[None]], axis=0).astype(f32)
-    pc = jnp.pad(pc, ((0, pc_rows - taps - 2), (0, 0)))
-    rate = -EXPONENT * jax.nn.softplus(-decay_param)
-    pr = jnp.concatenate([short_kernel.astype(f32), rate[None], initial_state[None]], axis=0)
-    pr_rows = -(-(short + 2) // 8) * 8
-    pr = jnp.pad(pr, ((0, pr_rows - short - 2), (0, 0)))
-    bd = jnp.stack([spread_heads(recur_map), spread_heads(input_map)])
-    sh = decay_shift.T.reshape(heads, tiles, 128).transpose(1, 0, 2)
-    sh = jnp.pad(sh, ((0, 0), (0, 8 - heads), (0, 0)))
+    wide = max(ca, cr)
+    pack_rows = -(-(short + 4) // 8) * 8
     vmem = pl.BlockSpec(memory_space=pltpu.VMEM)
     anyw = pl.BlockSpec(memory_space=pl.ANY)
     na, nu = n // 2, m // 2
@@ -1028,19 +1163,28 @@
     return pl.pallas_call(
         functools.partial(fused_kernel, n, m, dims),
         out_shape=jax.ShapeDtypeStruct((quarter, model), bf16),
-        in_specs=[vmem, vmem] + [anyw] * 10,
+        in_specs=[anyw] * 17,
         out_specs=vmem,
         scratch_shapes=[
+            pltpu.VMEM((quarter, model), bf16),
+            pltpu.VMEM((model,), bf16),
             pltpu.VMEM((quarter, model), bf16),
             pltpu.VMEM((m, quarter, model), bf16),
             pltpu.VMEM((n, depth, 2 * ca), bf16),
             pltpu.VMEM((n, depth, cr), bf16),
             pltpu.VMEM((n, depth, cr), bf16),
-            pltpu.VMEM((n, ca + cr, wid), bf16),
-            pltpu.VMEM((pc_rows, ca), f32),
-            pltpu.VMEM((pr_rows, cr), f32),
+            pltpu.VMEM((2, na, 2, ca + cr, wid // 2), bf16),
+            pltpu.VMEM(conv_kernel.shape, bf16),
+            pltpu.VMEM((ca,), bf16),
+            pltpu.VMEM((ca,), bf16),
+            pltpu.VMEM(short_kernel.shape, bf16),
+            pltpu.VMEM((2,) + recur_map.shape, bf16),
+            pltpu.VMEM((cr,), f32),
+            pltpu.VMEM((cr,), f32),
+            pltpu.VMEM((pack_rows, wide), f32),
+            pltpu.VMEM((-(-taps // 8) * 8, ca), f32),
             pltpu.VMEM((2, cr, cr), bf16),
-            pltpu.VMEM((tiles, 8, 128), f32),
+            pltpu.VMEM((heads, length), f32),
             pltpu.VMEM((ca // 128, pad + length, 128), f32),
             pltpu.VMEM((ca // 128, length, 128), f32),
             pltpu.VMEM((tiles, 8, 128), f32),
@@ -1055,13 +1199,13 @@
             pltpu.VMEM((length, cr), bf16),
             pltpu.VMEM((8, cr), f32),
             pltpu.VMEM((n, 8, cr), f32),
-            pltpu.VMEM((n, m, quarter, wid), bf16),
-            pltpu.VMEM((m, n, quarter, wid), bf16),
-            dma((6,)), dma((6,)), dma((4,)), dma((4,)),
-            dma((4, 2, na)), dma((4, na)), dma((4, na)), dma((4, na)),
-            dma((2,)), dma((2,)), dma((max(nu - 1, 1),)), dma((max(nu - 1, 1),)),
+            pltpu.VMEM((2, na, m, quarter, wid), bf16),
+            pltpu.VMEM((m, 2, na, quarter, wid), bf16),
+            dma((2,)), dma((8,)), dma((8,)), dma((9,)), dma((9,)),
+            dma((5, 2, na)), dma((5, na)), dma((5, na)), dma((5, na)),
+            dma((2,)), dma((2,)), dma((max(nu - 1, 1), 2)), dma((max(nu - 1, 1), 2)),
             dma((2,)), dma((2,)), dma((m - 1,)), dma((m - 1,)),
-            dma((n - 1,)), dma((n - 1,)), dma((n, m)), dma((n, m)), dma((1,)),
+            dma((n - 1,)), dma((n - 1,)), dma((2, na, m)), dma((2, na, m)),
         ],
         cost_estimate=pl.CostEstimate(
             flops=2 * length * (model * 2 * (ca + cr) + (ca + cr) * model), bytes_accessed=10_000_000,
@@ -1071,15 +1215,10 @@
             collective_id=7, has_side_effects=True, vmem_limit_bytes=60 * 1024 * 1024
         ),
     )(
-        tokens, norm_gain[None], conv_value_w, conv_gate_w, rnn_input_w, rnn_gate_w, conv_out_w, rnn_out_w,
-        pc, pr, bd, sh,
+        tokens, norm_gain, conv_value_w, conv_gate_w, rnn_input_w, rnn_gate_w, conv_out_w, rnn_out_w,
+        conv_kernel, conv_norm_gain, conv_norm_shift, short_kernel, recur_map, input_map, decay_param, initial_state,
+        decay_shift.T,
     )
-
-
-def spread_heads(maps):
-    heads, size, _ = maps.shape
-    rows = [jnp.pad(maps[h], ((0, 0), (h * size, (heads - 1 - h) * size))) for h in range(heads)]
-    return jnp.concatenate(rows, axis=0)
 
 
 def fits(n, m, args):
@@ -1089,7 +1228,7 @@
     wid = args[15].shape[1]
     heads = args[10].shape[0]
     return (
-        n % 2 == 0 and m % 2 == 0 and wid % 128 == 0 and ca % 256 == 0 and cr % 128 == 0 and depth % 16 == 0
+        n == 8 and m % 2 == 0 and wid % 256 == 0 and ca % 256 == 0 and cr % 128 == 0 and depth % 16 == 0
         and quarter % 32 == 0 and (quarter * m) % 256 == 0 and heads <= 8
     )
 

time: 166 us -> 142 us (0.86)
  Pallas kernels: 157 us -> 140 us
  local copies, waits for them, and re-layouts: 5.42 us -> 2.09 us
  other arithmetic: 2.98 us -> 0 us
    pallas_call x1, Pallas kernels: 157 us -> 140 us  [fused(): pl.pallas_call(functools.partial(fused_kernel, n, m, dims), out_shape=jax...]
    squeeze x2 -> x0, local copies, waits for them, and re-layouts: 2.06 us -> none  [spread_heads(): maps[h]]
    another operation x2 -> x0, other arithmetic: 1.7 us -> none  [fused(): bd = jnp.stack([spread_heads(recur_map), spread_heads(input_map)])]
where the time goes in v2:
time: 142 us
  Pallas kernels  140 us (99%)
  local copies, waits for them, and re-layouts  2.09 us (1%)
    pallas_call x1, Pallas kernels, fused(): pl.pallas_call(functools.partial(fused_kernel, n, m, dims), out_shape=jax...  140 us

profile of v2, /device:TPU:29, one launch (start us, length us, event | category | flops | bytes accessed | tf_op | source)
XLA Modules:
  0.0 141.8 jit_solution(17231745635422525161)
XLA Ops:
  0.0 139.7 %shard_map.163 = bf16[192,2048]{1,0:T(8,128)(2,1)} custom-call(bf16[192,2048]{1,0:T(8,128)(2,1)} %refs_0_.1, bf16[2048]{0:T(1024)(128)(2,1)} %refs_1_.1, bf16[256,512]{1,0:T(8,128)(2,1)} %refs_2_.1, bf16[256,512]{1,0:T(8,128)(2,1)} %refs_3_.1, bf16[256,640]{1,0:T(8,128)(2,1)} %refs_4_.1, bf16[256,640]{1,0:T(8,128)(2,1)} %refs_5_.1, ...), custom_call_target="tpu_custom_call" | custom-call | flops 10871635968 | bytes 10000000 | tf_op jit(solution)/shard_map/pallas_call | solution.py:1163
  139.7 2.1 %copy.19 = bf16[192,2048]{1,0:T(8,128)(2,1)} copy(bf16[192,2048]{1,0:T(8,128)(2,1)} %shard_map.163) | data formatting | bytes 1572864

commit v3 on v2

--- a/solution.py
+++ b/solution.py
@@ -403,20 +403,20 @@
         )
 
     barrier = pltpu.get_barrier_semaphore()
-    me = sp * m + tp
-
-    def greet(i, _):
-        to = (me + i) % (n * m)
-        pl.semaphore_signal(barrier, inc=1, device_id=at(to // m, to % m), device_id_type=pl.DeviceIdType.MESH)
-        return 0
-
     gets = [
         pltpu.make_async_copy(tok_ref, TB, own_sem.at[0]),
         pltpu.make_async_copy(ngain_hbm, NGB, own_sem.at[1]),
     ]
     for get in gets:
         get.start()
-    lax.fori_loop(1, n * m, greet, 0)
+    for i in range(n):
+        s_ = sp + i
+        s_ = jnp.where(s_ >= n, s_ - n, s_)
+        for j in range(m):
+            if i or j:
+                t_ = tp + j
+                t_ = jnp.where(t_ >= m, t_ - m, t_)
+                pl.semaphore_signal(barrier, inc=1, device_id=at(s_, t_), device_id_type=pl.DeviceIdType.MESH)
 
     hw = wid // 2
     bufs = [
@@ -475,6 +475,126 @@
             pltpu.make_async_copy(src, dst, par_recv.at[k]).start()
         pltpu.make_async_copy(sh_hbm, SH, par_recv.at[np_]).start()
 
+    pl.semaphore_wait(barrier, n * m - 1)
+
+    def param_send(k):
+        return remote(params[k][0], params[k][1], par_send.at[k], par_recv.at[k], sibling)
+
+    shift_send = remote(sh_hbm, SH, par_send.at[np_], par_recv.at[np_], partner)
+
+    tok_peer = remote(NB, X.at[tp], tok_send.at[0], tok_recv.at[v], at(2 * a + 1 - b, 2 * u + b))
+    tok_sib = remote(NB, X.at[tp], tok_send.at[1], tok_recv.at[v], sibling)
+
+    @pl.when(other)
+    def _():
+        bring_remote(0)
+
+    def block(s, o, core):
+        return bufs[s](o, core) if isinstance(s, int) else BO.at[s - 3, o, core]
+
+    def up(s, o):
+        ref = block(s, o, v)
+        return remote(ref, ref, line_send.at[s, 0, o], line_recv.at[s, o], at(2 * a + 2 + b, tp))
+
+    def down(s, o):
+        ref = block(s, o, v)
+        return remote(ref, ref, line_send.at[s, 1, o], line_recv.at[s, o], at(2 * a - 2 + b, tp))
+
+    def across(s, o, core):
+        ref = block(s, o, core)
+        return remote(ref, ref, sib_send.at[s, o], sib_recv.at[s, o], sibling)
+
+    low = a < na // 2
+
+    def inward(s, k, act):
+        @pl.when(jnp.logical_and(low, a - k >= 0))
+        def _():
+            act(up(s, a - k))
+
+        @pl.when(jnp.logical_and(jnp.logical_not(low), a + k < na))
+        def _():
+            act(down(s, a + k))
+
+    def outward(s, k, act):
+        @pl.when(jnp.logical_and(jnp.logical_and(low, a > 0), a + k < na))
+        def _():
+            act(down(s, a + k))
+
+        @pl.when(jnp.logical_and(jnp.logical_and(jnp.logical_not(low), a + 1 < na), a - k >= 0))
+        def _():
+            act(up(s, a - k))
+
+    window = 2
+    going_in, going_out = [], []
+
+    def push(way, order, s, k):
+        if len(order) >= window:
+            way(*order[-window], lambda c: c.wait_send())
+        way(s, k, lambda c: c.start())
+        order.append((s, k))
+
+    def push_in(s, k):
+        push(inward, going_in, s, k)
+
+    def push_out(s, k):
+        push(outward, going_out, s, k)
+
+    def hold(s):
+        brought(s)
+        across(s, a, v).start()
+
+    def take(s, k):
+        @pl.when(a - k >= 0)
+        def _():
+            up(s, a - k).wait_recv()
+            across(s, a - k, v).start()
+
+        @pl.when(a + k < na)
+        def _():
+            down(s, a + k).wait_recv()
+            across(s, a + k, v).start()
+
+    def crossed(s):
+        def one(o, _):
+            across(s, o, 1 - v).wait_recv()
+            return 0
+
+        lax.fori_loop(0, na, one, 0)
+
+    def tok_from(c):
+        q = 2 * u + c
+        return remote(NB, X.at[q], tok_send.at[0], tok_recv.at[c], sibling)
+
+    def tok_forward(i, uu, c):
+        ref = X.at[2 * uu + c]
+        return remote(ref, ref, tokf_send.at[i - 1, c], tokf_recv.at[i - 1, c], at(sp, 2 * ((u + i) % nu) + v))
+
+    at_end = jnp.logical_or(a == 0, a == na - 1)
+
+    def mids(f):
+        return pl.when(jnp.logical_not(at_end))(f)
+
+    def ends(f):
+        return pl.when(at_end)(f)
+
+    def token_relay(c):
+        @pl.when(jnp.logical_or(other, v != c))
+        def _():
+            tok_from(c).wait_recv()
+
+        for i in range(1, nu):
+            tok_forward(i, u, c).start()
+
+    def first_sends():
+        brought(0)
+        across(0, a, v).start()
+        inward(0, 0, lambda c: c.start())
+        outward(0, 0, lambda c: c.start())
+
+    @pl.when(same)
+    def _():
+        first_sends()
+
     for get in gets:
         get.wait()
     gain = NGB[...].astype(f32).reshape(1, model)
@@ -493,128 +613,18 @@
         return 0
 
     lax.fori_loop(0, quarter // 32, norm, 0)
-    pl.semaphore_wait(barrier, n * m - 1)
-
-    def param_send(k):
-        return remote(params[k][0], params[k][1], par_send.at[k], par_recv.at[k], sibling)
-
-    shift_send = remote(sh_hbm, SH, par_send.at[np_], par_recv.at[np_], partner)
-
-    tok_peer = remote(NB, X.at[tp], tok_send.at[0], tok_recv.at[v], at(2 * a + 1 - b, 2 * u + b))
-    tok_sib = remote(NB, X.at[tp], tok_send.at[1], tok_recv.at[v], sibling)
-
-    @pl.when(other)
-    def _():
-        bring_remote(0)
-
     @pl.when(same)
     def _():
         tok_peer.start()
         for k in range(np_):
             param_send(k).start()
 
-    def block(s, o, core):
-        return bufs[s](o, core) if isinstance(s, int) else BO.at[s - 3, o, core]
-
-    def up(s, o):
-        ref = block(s, o, v)
-        return remote(ref, ref, line_send.at[s, 0, o], line_recv.at[s, o], at(2 * a + 2 + b, tp))
-
-    def down(s, o):
-        ref = block(s, o, v)
-        return remote(ref, ref, line_send.at[s, 1, o], line_recv.at[s, o], at(2 * a - 2 + b, tp))
-
-    def across(s, o, core):
-        ref = block(s, o, core)
-        return remote(ref, ref, sib_send.at[s, o], sib_recv.at[s, o], sibling)
-
-    low = a < na // 2
-
-    def inward(s, k, act):
-        @pl.when(jnp.logical_and(low, a - k >= 0))
-        def _():
-            act(up(s, a - k))
-
-        @pl.when(jnp.logical_and(jnp.logical_not(low), a + k < na))
-        def _():
-            act(down(s, a + k))
-
-    def outward(s, k, act):
-        @pl.when(jnp.logical_and(jnp.logical_and(low, a > 0), a + k < na))
-        def _():
-            act(down(s, a + k))
-
-        @pl.when(jnp.logical_and(jnp.logical_and(jnp.logical_not(low), a + 1 < na), a - k >= 0))
-        def _():
-            act(up(s, a - k))
-
-    window = 2
-    going_in, going_out = [], []
-
-    def push(way, order, s, k):
-        if len(order) >= window:
-            way(*order[-window], lambda c: c.wait_send())
-        way(s, k, lambda c: c.start())
-        order.append((s, k))
-
-    def push_in(s, k):
-        push(inward, going_in, s, k)
-
-    def push_out(s, k):
-        push(outward, going_out, s, k)
-
-    def hold(s):
-        brought(s)
-        across(s, a, v).start()
-
-    def take(s, k):
-        @pl.when(a - k >= 0)
-        def _():
-            up(s, a - k).wait_recv()
-            across(s, a - k, v).start()
-
-        @pl.when(a + k < na)
-        def _():
-            down(s, a + k).wait_recv()
-            across(s, a + k, v).start()
-
-    def crossed(s):
-        def one(o, _):
-            across(s, o, 1 - v).wait_recv()
-            return 0
-
-        lax.fori_loop(0, na, one, 0)
-
-    def tok_from(c):
-        q = 2 * u + c
-        return remote(NB, X.at[q], tok_send.at[0], tok_recv.at[c], sibling)
-
-    def tok_forward(i, uu, c):
-        ref = X.at[2 * uu + c]
-        return remote(ref, ref, tokf_send.at[i - 1, c], tokf_recv.at[i - 1, c], at(sp, 2 * ((u + i) % nu) + v))
-
-    at_end = jnp.logical_or(a == 0, a == na - 1)
-
-    def mids(f):
-        return pl.when(jnp.logical_not(at_end))(f)
-
-    def ends(f):
-        return pl.when(at_end)(f)
-
-    def token_relay(c):
-        @pl.when(jnp.logical_or(other, v != c))
-        def _():
-            tok_from(c).wait_recv()
-
-        for i in range(1, nu):
-            tok_forward(i, u, c).start()
-
-    hold(0)
-    push_in(0, 0)
-    push_out(0, 0)
+    going_in.append((0, 0))
+    going_out.append((0, 0))
 
     @pl.when(other)
     def _():
+        first_sends()
         bring_remote(1)
         tok_sib.start()
         tok_peer.start()
@@ -1049,49 +1059,12 @@
 
         return ready, lambda: lax.fori_loop(0, 2, one, 0)
 
-    def outer(i, _):
-        ready, run = each_origin(i, produce)
-        ready()
-
-        @pl.when(jnp.logical_and(jnp.logical_not(at_end), i == na + 2))
-        def _():
-            take(4, 2)
-
-        run()
-
-        @mids
-        def _():
-            for stage, k in ((na - 1, 0), (na + 1, 1), (na + 2, 2)):
-
-                @pl.when(i == stage)
-                def _():
-                    push_out(4, k)
-
-        @pl.when(jnp.logical_and(at_end, i >= 1))
-        def _():
-            each_origin(i - 1, settle)[1]()
-
-        return 0
-
-    lax.fori_loop(0, 2 * na, outer, 0)
-
-    def conclude(i, _):
-        each_origin(i, settle)[1]()
-        return 0
-
-    lax.fori_loop(jnp.where(at_end, 2 * na - 1, 0), 2 * na, conclude, 0)
-
-    def drain(o, _):
-        for s in range(5):
+    def drain_early(o, _):
+        for s in range(3):
             across(s, o, v).wait_send()
         return 0
 
-    assert len(going_in) == 10 and len(going_out) == 15
-    lax.fori_loop(0, na, drain, 0)
-
-    for way, order in ((inward, going_in), (outward, going_out)):
-        for one in order[-window:]:
-            way(*one, lambda c: c.wait_send())
+    lax.fori_loop(0, na, drain_early, 0)
 
     @pl.when(other)
     def _():
@@ -1122,6 +1095,50 @@
         @pl.when(spc + i < n)
         def _():
             state_to(i).wait_send()
+
+    def outer(i, _):
+        ready, run = each_origin(i, produce)
+        ready()
+
+        @pl.when(jnp.logical_and(jnp.logical_not(at_end), i == na + 2))
+        def _():
+            take(4, 2)
+
+        run()
+
+        @mids
+        def _():
+            for stage, k in ((na - 1, 0), (na + 1, 1), (na + 2, 2)):
+
+                @pl.when(i == stage)
+                def _():
+                    push_out(4, k)
+
+        @pl.when(jnp.logical_and(at_end, i >= 3))
+        def _():
+            each_origin(i - 3, settle)[1]()
+
+        return 0
+
+    lax.fori_loop(0, 2 * na, outer, 0)
+
+    def conclude(i, _):
+        each_origin(i, settle)[1]()
+        return 0
+
+    lax.fori_loop(jnp.where(at_end, 2 * na - 3, 0), 2 * na, conclude, 0)
+
+    def drain(o, _):
+        for s in range(3, 5):
+            across(s, o, v).wait_send()
+        return 0
+
+    assert len(going_in) == 10 and len(going_out) == 15
+    lax.fori_loop(0, na, drain, 0)
+
+    for way, order in ((inward, going_in), (outward, going_out)):
+        for one in order[-window:]:
+            way(*one, lambda c: c.wait_send())
 
     def drain_out(o, _):
         for e in range(2):

time: 142 us -> 141 us (level); the launches traced: 142 us -> 139 us
  Pallas kernels: 140 us -> 137 us
    pallas_call x1, Pallas kernels: 140 us -> 137 us  [fused(): pl.pallas_call(functools.partial(fused_kernel, n, m, dims), out_shape=jax...]
where the time goes in v3:
time: 141 us; the launch traced here: 139 us
  Pallas kernels  137 us (97%)
  local copies, waits for them, and re-layouts  2.09 us (1%)
    pallas_call x1, Pallas kernels, fused(): pl.pallas_call(functools.partial(fused_kernel, n, m, dims), out_shape=jax...  137 us

profile of v3, /device:TPU:29, one launch (start us, length us, event | category | flops | bytes accessed | tf_op | source)
XLA Modules:
  0.0 139.2 jit_solution(16855042743945103443)
XLA Ops:
  0.0 137.1 %shard_map.163 = bf16[192,2048]{1,0:T(8,128)(2,1)} custom-call(bf16[192,2048]{1,0:T(8,128)(2,1)} %refs_0_.1, bf16[2048]{0:T(1024)(128)(2,1)} %refs_1_.1, bf16[256,512]{1,0:T(8,128)(2,1)} %refs_2_.1, bf16[256,512]{1,0:T(8,128)(2,1)} %refs_3_.1, bf16[256,640]{1,0:T(8,128)(2,1)} %refs_4_.1, bf16[256,640]{1,0:T(8,128)(2,1)} %refs_5_.1, ...), custom_call_target="tpu_custom_call" | custom-call | flops 10871635968 | bytes 10000000 | tf_op jit(solution)/shard_map/pallas_call | solution.py:1180
  137.2 2.1 %copy.19 = bf16[192,2048]{1,0:T(8,128)(2,1)} copy(bf16[192,2048]{1,0:T(8,128)(2,1)} %shard_map.163) | data formatting | bytes 1572864
